TPU v7x, 512 devices: a whole 4x8x8 slice. The times are simulated.
512 devices in a mesh: ep: 32 (over z, x), tp: 16 (over y, core).
Axes of the slice: x: 4, y: 8, z: 8, core: 2. Of those that a mesh axis runs over, the one named last changes fastest.
Arguments:
- tokens: bfloat16 [256, 2048], P('ep', 'tp'), may hold values from -10 to 10, as said below
- norm_gain: float32 [2048], P('tp'), may hold values from 0.5 to 1.5
- norm_bias: float32 [2048], P('tp'), may hold values from -0.3 to 0.3
- group_pick: int32 [256, 1], P('ep'), may hold values from 0 to 7; in each aligned block of 8 rows (0 to 7, 8 to 15, ...) at most 2 rows name the same one
- member_pick: int32 [256, 4], P('ep'), may hold values from 0 to 7, all different within a row
- picked_probs: float32 [256, 4], P('ep'), may hold values from 0.05 to 1
- gate_weight: bfloat16 [64, 2048, 1024], P('ep', 'tp'), may hold values from -0.125 to 0.125
- up_weight: bfloat16 [64, 2048, 1024], P('ep', 'tp'), may hold values from -0.125 to 0.125
- down_weight: bfloat16 [64, 1024, 2048], P('ep', None, 'tp'), may hold values from -0.375 to 0.375
Outputs:
- mixed: bfloat16 [256, 2048], P('ep', 'tp')
Inputs may be any that keep to these rules, and one draw needn't show every extreme that they name: `group_pick`: each entry is a group number from 0 to 7; within each aligned block of 8 tokens no group is named by more than 2 tokens, a bound that some block reaches. `member_pick`: each token's 4 entries are different member numbers from 0 to 7. `tokens`: each token is its own offset between -2 and 2 plus its own scale between 0.25 and 2 times entries of at most 4 in size.
All inputs are finite; a program needn't handle non-finite values.
Results may differ from a plain program's by a relative error of at most 0.01.
Values may be sent and summed in bfloat16 or wider, within the bound.
A program may use at most 64 MiB of HBM per device.

v0:
```python
import functools

import jax
import jax.numpy as jnp
from jax import lax
from jax.sharding import Mesh
from jax.sharding import PartitionSpec as P

EPG = 8
TP = ("tp_0", "tp_1")


norm_epsilon = 1e-05


def together(arrays, axis):
    ends = [0]
    for a in arrays:
        ends.append(ends[-1] + a.size)
    subtotal = lax.psum(jnp.concatenate([a.ravel() for a in arrays]), axis)
    return tuple(subtotal[b:e].reshape(a.shape) for a, b, e in zip(arrays, ends, ends[1:]))


def one_axis_at_a_time(x, axes):
    return functools.reduce(lax.psum, axes, x)


def normalize(tokens, norm_gain, norm_bias):
    values = tokens.astype(jnp.float32)
    features = values.shape[1] * lax.axis_size(TP)
    first_sums, square_sums = together(
        (jnp.sum(values, axis=1, keepdims=True), jnp.sum(values * values, axis=1, keepdims=True)),
        TP,
    )
    center = first_sums / features
    shifted = values - center
    spread = square_sums / features - center * center
    scaled = shifted * lax.rsqrt(spread + norm_epsilon)
    return (scaled * norm_gain.astype(jnp.float32) + norm_bias.astype(jnp.float32)).astype(
        jnp.bfloat16
    )


def membership(labels, number):
    levels = lax.broadcasted_iota(jnp.int32, (1, 1, number), 2)
    return jnp.any(labels[:, :, None] == levels, axis=1).astype(jnp.int32)


def earlier_counts(present):
    return (jnp.cumsum(present, axis=0) - present).astype(jnp.int32)


def placement(present, slots, capacity):
    levels = lax.broadcasted_iota(jnp.int32, (1, 1, capacity), 2)
    hits = present[:, :, None] * (slots[:, :, None] == levels).astype(jnp.int32)
    return hits.reshape(present.shape[0], -1).astype(jnp.bfloat16)


def pack_rows(placed, normed):
    return jnp.einsum("tp,td->pd", placed, normed, preferred_element_type=jnp.float32).astype(
        jnp.bfloat16
    )


def activate(gate_full, up_full):
    return (jax.nn.silu(gate_full) * up_full).astype(jnp.bfloat16)


def project_down(hidden, down_weight):
    return jnp.einsum(
        "jrf,jfd->jrd", hidden, down_weight, preferred_element_type=jnp.float32
    ).astype(jnp.bfloat16)


def by_source(results, peers, capacity):
    local_experts = results.shape[0]
    width = results.shape[2]
    parted = results.reshape(local_experts, peers, capacity, width)
    return jnp.transpose(parted, (1, 0, 2, 3)).reshape(peers, local_experts * capacity, width)


def combine(returned, positions, shares):
    picked = jnp.take(returned, positions, axis=0)
    return jnp.sum(shares[:, :, None] * picked.astype(jnp.float32), axis=1).astype(jnp.bfloat16)


def on_device(
    tokens,
    norm_gain,
    norm_bias,
    group_pick,
    member_pick,
    picked_probs,
    gate_weight,
    up_weight,
    down_weight,
):
    normed = normalize(tokens, norm_gain, norm_bias)
    token_count = tokens.shape[0]
    shard_width = tokens.shape[1]
    local_experts = gate_weight.shape[0]
    peers = lax.axis_size("ep")
    experts = local_experts * peers
    groups = experts // EPG
    capacity = max(token_count // 4, (token_count + groups - 1) // groups)
    chosen = (group_pick * EPG + member_pick).astype(jnp.int32)
    shares = picked_probs / jnp.sum(picked_probs, axis=1, keepdims=True)
    present = membership(chosen, experts)
    slots = earlier_counts(present)
    outgoing = pack_rows(placement(present, slots, capacity), normed)
    outgoing = outgoing.reshape(peers, local_experts * capacity, shard_width)
    incoming = lax.all_to_all(outgoing, "ep", split_axis=0, concat_axis=0, tiled=True)
    rows = incoming.reshape(peers, local_experts, capacity, shard_width)
    rows = jnp.transpose(rows, (1, 0, 2, 3)).reshape(local_experts, peers * capacity, shard_width)
    gate_part = jnp.einsum("jrd,jdf->jrf", rows, gate_weight, preferred_element_type=jnp.float32)
    up_part = jnp.einsum("jrd,jdf->jrf", rows, up_weight, preferred_element_type=jnp.float32)
    gate_full, up_full = (one_axis_at_a_time(gate_part, TP), one_axis_at_a_time(up_part, TP))
    results = project_down(activate(gate_full, up_full), down_weight)
    returned = lax.all_to_all(
        by_source(results, peers, capacity), "ep", split_axis=0, concat_axis=0, tiled=True
    )
    positions = chosen * capacity + jnp.take_along_axis(slots, chosen, axis=1)
    mixed = combine(returned.reshape(experts * capacity, shard_width), positions, shares)
    return mixed


def solution(mesh):
    finer = Mesh(mesh.devices.reshape(mesh.shape["ep"], 8, 2), ("ep", "tp_0", "tp_1"))
    placed = (
        P("ep", TP),
        P(TP),
        P(TP),
        P("ep", None),
        P("ep", None),
        P("ep", None),
        P("ep", TP, None),
        P("ep", TP, None),
        P("ep", None, TP),
    )
    return jax.shard_map(
        on_device, mesh=finer, in_specs=placed, out_specs=P("ep", TP), check_vma=False
    )
```

profile of v0, /device:TPU:1, one launch (start us, length us, event | category | flops | bytes accessed | tf_op | source)
XLA Modules:
  0.0 202.2 jit_solution(17553658940312224399)
XLA Ops:
  6.5 0.0 copy-start
  6.5 0.0 all-reduce.5.cloned.1.call-start
  6.5 0.7 multiply_bitcast_fusion
  7.3 0.8 convert_reduce_fusion
  8.1 0.1 pad_maximum_fusion
  8.2 29.8 %psum.35 = f32[16]{0:T(128)S(1)} all-reduce(f32[16]{0:T(128)S(1)} %pad_maximum_fusion), channel_id=1, replica_groups=mesh['ep'=32,'tp_0'=8,'tp_1'=2] {'tp_0','tp_1'}, use_global_device_ids=true, to_apply=%region_5.0 | all-reduce | flops 16 | bytes 128 | tf_op jit(solution)/shard_map/psum | solution.py:20
  38.0 0.1 slice_multiply_fusion
  38.1 0.0 copy-done.3
  38.1 0.1 copy.34
  38.2 0.1 clamp_shift-left_fusion
  38.2 0.1 copy.35
  38.3 0.1 fusion.2
  38.4 0.1 copy.39
  38.5 0.1 copy.38
  38.6 0.1 eq.39
  38.8 0.0 copy-start.4
  38.8 0.0 copy-start.6
  38.8 0.0 copy-start.7
  38.9 0.6 copy-done.4
  39.5 0.0 copy-done.6
  39.5 0.0 copy-done.7
  39.5 0.2 convolution_convert_fusion.1
  39.7 16.6 %all_to_all.10 = bf16[32,4,128]{2,1,0:T(4,128)(2,1)S(1)} all-to-all(bf16[32,4,128]{2,1,0:T(4,128)(2,1)S(1)} %bitcast.32), channel_id=1, replica_groups=mesh['ep'=32,'tp_0'=8,'tp_1'=2] {'ep'}, dimensions={0} | all-to-all | bytes 65536 | tf_op jit(solution)/shard_map/all_to_all | solution.py:112
  56.4 0.0 copy-done
  56.4 0.0 copy-start.1
  56.4 1.0 fusion.16
  57.4 0.0 copy-done.1
  57.5 1.0 fusion.15
  58.5 0.0 all-reduce.5.cloned.1.call-update
  58.5 0.0 all-reduce.7.cloned.1.call-start
  58.6 71.8 %all-reduce.5.cloned.1.call-done = (f32[2,64,1024]{2,1,0:T(8,128)}, f32[2,64,1024]{2,1,0:T(8,128)}) async-done(((f32[2,64,1024]{2,1,0:T(8,128)}, f32[2,64,1024]{2,1,0:T(8,128)}), (f32[2,64,1024]{2,1,0:T(8,128)}, f32[2,64,1024]{2,1,0:T(8,128)})) %all-reduce.5.cloned.1.call-update) | async-done | bytes 1048592 | tf_op jit(solution)/shard_map/psum | solution.py:25
  130.4 0.0 all-reduce.7.cloned.1.call-update
  130.4 0.7 copy-done.2
  131.1 0.1 copy.33
  131.2 0.1 copy.36
  131.3 0.1 copy.37
  131.4 0.1 reshape.74
  131.4 0.7 gather_fusion.1
  132.1 0.1 reshape.77
  132.2 0.1 reshape.68
  132.3 42.1 %all-reduce.7.cloned.1.call-done = (f32[2,64,1024]{2,1,0:T(8,128)}, f32[2,64,1024]{2,1,0:T(8,128)}) async-done(((f32[2,64,1024]{2,1,0:T(8,128)}, f32[2,64,1024]{2,1,0:T(8,128)}), (f32[2,64,1024]{2,1,0:T(8,128)}, f32[2,64,1024]{2,1,0:T(8,128)})) %all-reduce.7.cloned.1.call-update) | async-done | bytes 1048592 | tf_op jit(solution)/shard_map/psum | solution.py:25
  174.4 0.0 copy-done.5
  174.4 1.5 convolution_convert_fusion
  175.9 0.6 copy.42
  176.5 8.9 %all-to-all-start.1 = ((bf16[32,4,128]{2,1,0:T(4,128)(2,1)}), bf16[32,4,128]{2,1,0:T(4,128)(2,1)S(1)}, u32[]{:S(2)}, u32[]{:S(2)}) async-start(bf16[32,4,128]{2,1,0:T(4,128)(2,1)} %copy.42), calls=%async_computation.1 | async-start | bytes 65536 | tf_op jit(solution)/shard_map/all_to_all | solution.py:119
  185.4 8.6 %all-to-all-done.1 = bf16[32,4,128]{2,1,0:T(4,128)(2,1)S(1)} async-done(((bf16[32,4,128]{2,1,0:T(4,128)(2,1)}), bf16[32,4,128]{2,1,0:T(4,128)(2,1)S(1)}, u32[]{:S(2)}, u32[]{:S(2)}) %all-to-all-start.1) | async-done | bytes 32800 | tf_op jit(solution)/shard_map/all_to_all | solution.py:119
  194.0 0.6 gather_fusion
  194.6 0.7 multiply_reduce_fusion
  (16 shorter events, 0.2 us)
Async XLA Ops:
  6.5 49.9 %copy-start = (bf16[2,128,1024]{2,1,0:T(8,128)(2,1)S(1)}, bf16[2,128,1024]{2,1,0:T(8,128)(2,1)}, u32[]{:S(2)}) copy-start(bf16[2,128,1024]{2,1,0:T(8,128)(2,1)} %param.16) | copy-start | bytes 1572868
  6.5 123.8 %all-reduce.5.cloned.1.call-start = ((), (), s32[]{:S(2)}) async-start(), calls=%async_computation.2 | async-start | bytes 2097152 | tf_op jit(solution)/shard_map/psum | solution.py:25
  8.2 29.9 %copy-start.3 = (s32[8,4]{0,1:T(4,128)S(1)}, s32[8,4]{0,1:T(4,128)}, u32[]{:S(2)}) copy-start(s32[8,4]{0,1:T(4,128)} %param.13) | copy-start | bytes 388
  38.8 0.7 copy-start.4
  38.8 0.7 copy-start.6
  38.8 0.7 copy-start.7
  56.4 1.1 copy-start.1
  58.5 115.9 %all-reduce.7.cloned.1.call-start = ((), (), s32[]{:S(2)}) async-start(), calls=%async_computation.3 | async-start | bytes 2097152 | tf_op jit(solution)/shard_map/psum | solution.py:25
  130.4 0.7 copy-start.2
  131.4 42.9 %copy-start.5 = (bf16[2,1024,128]{2,1,0:T(8,128)(2,1)S(1)}, bf16[2,1024,128]{2,1,0:T(8,128)(2,1)}, u32[]{:S(2)}) copy-start(bf16[2,1024,128]{2,1,0:T(8,128)(2,1)} %param.17) | copy-start | bytes 1572868
  176.5 17.5 %all-to-all-start.1 = ((bf16[32,4,128]{2,1,0:T(4,128)(2,1)}), bf16[32,4,128]{2,1,0:T(4,128)(2,1)S(1)}, u32[]{:S(2)}, u32[]{:S(2)}) async-start(bf16[32,4,128]{2,1,0:T(4,128)(2,1)} %copy.42), calls=%async_computation.1 | async-start | bytes 65536 | tf_op jit(solution)/shard_map/all_to_all | solution.py:119
Sparse Core Ops, SparseCore 0:
  58.6 71.7 all-reduce.4
  133.3 41.0 all-reduce.6
where the time goes:
time: 203 us; the launch traced here: 202 us
  waiting for transfers between devices  123 us (61%)
  blocking collectives  46.5 us (23%)
  between operations  13.5 us (7%)
  starting transfers between devices  8.95 us (4%)
  local copies, waits for them, and re-layouts  4.28 us (2%)
  matrix products  3.75 us (2%)
  other arithmetic  2.62 us (1%)
    psum x2, waiting for transfers between devices, one_axis_at_a_time(): return functools.reduce(lax.psum, axes, x)  114 us
    psum x1, blocking collectives, together(): subtotal = lax.psum(jnp.concatenate([a.ravel() for a in arrays]), axis)  29.8 us
    all_to_all x1, blocking collectives, on_device(): lax.all_to_all(outgoing, 'ep', split_axis=0, concat_axis=0, tiled=True)  16.6 us
    all_to_all x1, starting transfers between devices, on_device(): lax.all_to_all(by_source(results, peers, capacity), 'ep', split_axis=0, c...  8.9 us
    all_to_all x1, waiting for transfers between devices, on_device(): lax.all_to_all(by_source(results, peers, capacity), 'ep', split_axis=0, c...  8.62 us
  transfers between devices with their start and end apart: 3, of which 3 were waited for; matrix products, arithmetic and copies ran while one was open for 1% of the time, Pallas kernels for 0%

commit v1 on v0

v1 whole, which is shorter than its diff:
```python
import functools

import jax
import jax.numpy as jnp
from jax import lax
from jax.experimental import pallas as pl
from jax.experimental.pallas import tpu as pltpu
from jax.sharding import PartitionSpec as P

EPG = 8
CAP = 2
norm_epsilon = 1e-05
MESH = pl.DeviceIdType.MESH
F32 = jnp.float32
BF16 = jnp.bfloat16
L = 128


def iota(shape, axis):
    return lax.broadcasted_iota(jnp.int32, shape, axis)


def far_first(n):
    return sorted(range(1, n), key=lambda d: -min(d, n - d))


def kernel(
    nz, nx, ny, features,
    tok_ref, gain_ref, bias_ref, gp_ref, mp_ref, pp_ref, gate_ref, up_ref, down_ref,
    out_ref,
    wg, wu, wd, gb,
    s1, r1, r2t, r2s, ax1s, ax1r, ax2s, ax2r, ps, pr, hb, o5s, r5, s6, r6,
    lsem, xsem_s, xsem_r, s1s, s1r, s2s_s, s2s_r, s2t_s, s2t_r, a1s, a1r, a2s, a2r,
    p_s, p_r, h_s, h_r, o_s, o_r, f_s, f_r,
):
    tokens = tok_ref.shape[0]
    half = wg.shape[2]
    rows = nz * CAP
    per_expert = ny // 2
    ep, tp = lax.axis_index("ep"), lax.axis_index("tp")
    z, x, y, c = ep // nx, ep % nx, tp // 2, tp % 2

    def dev(dz=0, dx=0, dy=0, dc=0):
        return {
            "ep": ((z + dz + nz) % nz) * nx + (x + dx + nx) % nx,
            "tp": ((y + dy + ny) % ny) * 2 + (c + dc) % 2,
        }

    def remote(src, dst, ss, rs, device):
        return pltpu.make_async_remote_copy(
            src_ref=src, dst_ref=dst, send_sem=ss, recv_sem=rs, device_id=device, device_id_type=MESH
        )

    def each(n, body):
        lax.fori_loop(1, n, lambda d, carry: (body(d), carry)[1], 0)

    mine = pl.ds(pl.multiple_of(c * half, half), half)
    other = pl.ds(pl.multiple_of((1 - c) * half, half), half)
    local = [
        pltpu.make_async_copy(gate_ref.at[:, :, mine], wg.at[:, 0:L, :], lsem.at[0]),
        pltpu.make_async_copy(up_ref.at[:, :, mine], wu.at[:, 0:L, :], lsem.at[1]),
        pltpu.make_async_copy(down_ref.at[:, mine, :], wd.at[:, :, 0:L], lsem.at[2]),
    ]
    for copy in local:
        copy.start()

    barrier = pltpu.get_barrier_semaphore()

    def greet(**where):
        pl.semaphore_signal(barrier, inc=1, device_id=dev(**where), device_id_type=MESH)

    each(nz, lambda d: greet(dz=d))
    each(ny, lambda d: greet(dy=d))
    each(2 * nx, lambda k: greet(dx=k // 2, dc=k % 2))

    group = (gp_ref[...] - z + nz) % nz
    lane = iota((tokens, L), 1)
    member = (group == lane // CAP).astype(F32)
    count = jnp.zeros((tokens, L), F32)
    sub = iota((tokens, L), 0)
    for t in range(tokens - 1):
        count = count + jnp.where(sub > t, member[t : t + 1, :], 0.0)
    chosen = member * (count == (lane % CAP).astype(F32)).astype(F32)
    probs = pp_ref[...]
    share = probs / jnp.sum(probs, axis=1, keepdims=True)
    high = share.astype(BF16).astype(F32)
    low = share - high
    picks = mp_ref[...]
    shares = jnp.zeros((tokens, L), F32)
    for k in range(picks.shape[1]):
        pick = picks[:, k : k + 1]
        shares = shares + jnp.where(lane == pick, high[:, k : k + 1], 0.0)
        shares = shares + jnp.where(lane == pick + EPG, low[:, k : k + 1], 0.0)
    rowwise = jnp.transpose(chosen)[0:rows, :]
    both = jnp.concatenate([tok_ref[...].astype(F32), shares], axis=1)
    packed = jnp.zeros((rows, 2 * L), F32)
    for t in range(tokens):
        packed = packed + rowwise[:, t : t + 1] * both[t : t + 1, :]
    for d in range(nz):
        s1[d] = packed[d * CAP : (d + 1) * CAP, :]
    r1[0] = packed[0:CAP, :]

    pl.semaphore_wait(barrier, (nz - 1) + (ny - 1) + (2 * nx - 1))

    def s1_copy(d):
        return remote(s1.at[d], r1.at[d], s1s.at[d], s1r.at[d], dev(dz=d))

    each(nz, lambda d: s1_copy(d).start())

    def swaps():
        to = dev(dc=1)
        return [
            remote(gate_ref.at[:, :, other], wg.at[:, L : 2 * L, :], xsem_s.at[0], xsem_r.at[0], to),
            remote(up_ref.at[:, :, other], wu.at[:, L : 2 * L, :], xsem_s.at[1], xsem_r.at[1], to),
            remote(down_ref.at[:, other, :], wd.at[:, :, L : 2 * L], xsem_s.at[2], xsem_r.at[2], to),
            remote(gain_ref, gb.at[0], xsem_s.at[3], xsem_r.at[3], to),
            remote(bias_ref, gb.at[1], xsem_s.at[4], xsem_r.at[4], to),
        ]

    for copy in swaps():
        copy.start()

    each(nz, lambda d: s1_copy(d).wait_recv())

    block = jnp.concatenate([r1[d] for d in range(nz)], axis=0)
    r2t[0, 0] = block[:, 0:L].astype(BF16)
    r2s[0] = block[:, L : 2 * L].astype(BF16)

    def s2_copy(k):
        dx, dc = k // 2, k % 2
        return remote(r2t.at[0, 0], r2t.at[dx, dc], s2t_s.at[k], s2t_r.at[k], dev(dx=dx, dc=dc))

    def s2_shares(dx):
        return remote(r2s.at[0], r2s.at[dx], s2s_s.at[dx], s2s_r.at[dx], dev(dx=dx))

    each(2 * nx, lambda k: s2_copy(k).start())
    each(nx, lambda k: s2_shares(k).start())

    for copy in local:
        copy.wait()
    for copy in swaps():
        copy.wait()
    gain = jnp.concatenate([gain_ref[...], gb[0]], axis=1)
    bias = jnp.concatenate([bias_ref[...], gb[1]], axis=1)
    gain_high = gain.astype(BF16).astype(F32)
    bias_high = bias.astype(BF16).astype(F32)
    four = iota((16, 2 * L), 0)
    vectors = jnp.where(four == 0, gain_high, 0.0) + jnp.where(four == 1, gain - gain_high, 0.0)
    vectors = vectors + jnp.where(four == 2, bias_high, 0.0) + jnp.where(four == 3, bias - bias_high, 0.0)
    vectors = vectors.astype(BF16)
    for e in range(2):
        for side, weight in enumerate((wg, wu)):
            line = jnp.dot(vectors, weight[e], preferred_element_type=F32)
            for j in range(per_expert):
                part = line[:, j * L : (j + 1) * L]
                ax1s[e * per_expert + j, 0:1, side * L : (side + 1) * L] = part[0:1] + part[1:2]
                ax1s[e * per_expert + j, 1:2, side * L : (side + 1) * L] = part[2:3] + part[3:4]
    ax1r[0] = ax1s[y]

    def a1_copy(d):
        return remote(ax1s.at[(y + d) % ny], ax1r.at[d], a1s.at[d], a1r.at[d], dev(dy=d))

    each(ny, lambda d: a1_copy(d).start())

    each(2 * nx, lambda k: s2_copy(k).wait_recv())

    all_rows = nx * rows
    own = jnp.concatenate([r2t[dx, 0] for dx in range(nx)], axis=0).astype(F32)
    partner = jnp.concatenate([r2t[dx, 1] for dx in range(nx)], axis=0).astype(F32)
    middle = jnp.sum(own + partner, axis=1, keepdims=True) * (1.0 / (2 * L))
    own = own - middle
    partner = partner - middle
    scaled = jnp.concatenate([own * gain[:, 0:L], partner * gain[:, L : 2 * L]], axis=1).astype(BF16)

    def p_copy(d):
        return remote(ps.at[d], pr.at[d], p_s.at[d], p_r.at[d], dev(dy=d))

    def a2_copy(d):
        return remote(ax2s, ax2r.at[d], a2s.at[d], a2r.at[d], dev(dy=d))

    gate_own = up_own = None
    for place, d in enumerate(far_first(ny) + [0]):
        q = (y + d) % ny
        e = q // per_expert
        cols = pl.ds(pl.multiple_of((q % per_expert) * L, L), L)
        gate_part = jnp.dot(scaled, wg[e, :, cols], preferred_element_type=F32)
        up_part = jnp.dot(scaled, wu[e, :, cols], preferred_element_type=F32)
        if d == 0:
            gate_own, up_own = gate_part, up_part
        else:
            ps[d, 0] = gate_part.astype(BF16)
            ps[d, 1] = up_part.astype(BF16)
            p_copy(d).start()
        if place == 2 or (place == 0 and ny == 2):
            squares = jnp.sum(own * own + partner * partner, axis=1, keepdims=True)
            lanes = iota((all_rows, L), 1)
            columns = jnp.where(lanes == 0, middle, 0.0) + jnp.where(lanes == 1, squares, 0.0)
            turned = jnp.transpose(columns)
            ax2s[:, 0:all_rows] = turned[0:2, :]
            ax2r[0, :, 0:all_rows] = turned[0:2, :]
            each(ny, lambda d: a2_copy(d).start())

    each(ny, lambda d: a1_copy(d).wait_recv())
    each(ny, lambda d: a2_copy(d).wait_recv())
    means = [ax2r[d, 0:1, 0:all_rows] for d in range(ny)]
    center = sum(means) * (1.0 / ny)
    shifts = [m - center for m in means]
    spread = sum(ax2r[d, 1:2, 0:all_rows] for d in range(ny)) + (features // ny) * sum(s * s for s in shifts)
    scale = lax.rsqrt(spread * (1.0 / features) + norm_epsilon)
    depth = 16
    stack = iota((depth, all_rows), 0)
    table = jnp.where(stack == ny, scale, 0.0)
    for d in range(ny):
        table = table + jnp.where(stack == d, shifts[d], 0.0)
    table = jnp.transpose(table)
    scale = table[:, ny : ny + 1]
    gate, up = gate_own, up_own
    gate_bias = up_bias = jnp.zeros((1, L), F32)
    for d in range(ny):
        shift = table[:, d : d + 1]
        gate = gate + shift * ax1r[d, 0:1, 0:L]
        up = up + shift * ax1r[d, 0:1, L : 2 * L]
        gate_bias = gate_bias + ax1r[d, 1:2, 0:L]
        up_bias = up_bias + ax1r[d, 1:2, L : 2 * L]
    each(nx, lambda k: s2_shares(k).wait_recv())
    expert = 2 * x + y // per_expert
    lanes = iota((all_rows, L), 1)
    share = jnp.concatenate([r2s[dx] for dx in range(nx)], axis=0).astype(F32)
    share = jnp.sum(
        jnp.where((lanes == expert) | (lanes == expert + EPG), share, 0.0), axis=1, keepdims=True
    )

    for d in sorted(range(1, ny), key=lambda d: min(d, ny - d)):
        p_copy(d).wait_recv()
        gate = gate + pr[d, 0].astype(F32)
        up = up + pr[d, 1].astype(F32)
    gate = gate * scale + gate_bias
    up = up * scale + up_bias
    hidden = (share * (gate / (1.0 + jnp.exp(-gate)) * up)).astype(BF16)
    hb[0] = hidden

    def h_copy(d):
        return remote(hb.at[0], hb.at[d], h_s.at[d], h_r.at[d], dev(dy=d))

    for d in far_first(ny):
        h_copy(d).start()

    def down(d):
        q = (y - d + ny) % ny
        units = pl.ds(pl.multiple_of((q % per_expert) * L, L), L)
        return jnp.dot(hb[d], wd[q // per_expert, units, :], preferred_element_type=F32)

    total = down(0)
    for d in sorted(range(1, ny), key=lambda d: min(d, ny - d)):
        h_copy(d).wait_recv()
        total = total + down(d)

    for dx in range(nx):
        for dc in range(2):
            o5s[dx, dc] = total[dx * rows : (dx + 1) * rows, dc * L : (dc + 1) * L].astype(BF16)

    def o_copy(k):
        dx, dc = k // 2, k % 2
        return remote(o5s.at[dx, dc], r5.at[dx, dc], o_s.at[k], o_r.at[k], dev(dx=-dx, dc=dc))

    each(2 * nx, lambda k: o_copy(k).start())
    summed = total[0:rows, 0:L]
    each(2 * nx, lambda k: o_copy(k).wait_recv())
    for k in range(1, 2 * nx):
        summed = summed + r5[k // 2, k % 2].astype(F32)
    summed = summed.astype(BF16).astype(F32)

    for d in range(nz):
        s6[d] = summed[d * CAP : (d + 1) * CAP, :]
    r6[0] = summed[0:CAP, :]

    def f_copy(d):
        return remote(s6.at[d], r6.at[d], f_s.at[d], f_r.at[d], dev(dz=-d))

    each(nz, lambda d: f_copy(d).start())

    each(nz, lambda d: s1_copy(d).wait_send())
    each(2 * nx, lambda k: s2_copy(k).wait_send())
    each(nx, lambda k: s2_shares(k).wait_send())
    each(ny, lambda d: a1_copy(d).wait_send())
    each(ny, lambda d: a2_copy(d).wait_send())
    each(ny, lambda d: p_copy(d).wait_send())
    each(ny, lambda d: h_copy(d).wait_send())
    each(2 * nx, lambda k: o_copy(k).wait_send())
    each(nz, lambda d: f_copy(d).wait_send())
    each(nz, lambda d: f_copy(d).wait_recv())

    result = jnp.zeros((tokens, L), F32)
    for d in range(nz):
        back = r6[d]
        for s in range(CAP):
            at = d * CAP + s
            result = result + chosen[:, at : at + 1] * back[s : s + 1, :]
    out_ref[...] = result.astype(BF16)


def solution(mesh):
    nx = EPG // 2
    nz = mesh.shape["ep"] // nx
    ny = mesh.shape["tp"] // 2

    def on_device(tokens, gain, bias, group_pick, member_pick, probs, gate, up, down):
        width = tokens.shape[1]
        half = gate.shape[2] // 2
        rows = nz * CAP
        all_rows = nx * rows
        vmem, dma = pltpu.VMEM, pltpu.SemaphoreType.DMA
        whole = pl.BlockSpec(memory_space=pltpu.VMEM)
        away = pl.BlockSpec(memory_space=pl.ANY)
        return pl.pallas_call(
            functools.partial(kernel, nz, nx, ny, width * 2 * ny),
            out_shape=jax.ShapeDtypeStruct(tokens.shape, BF16),
            in_specs=[whole] * 6 + [away] * 3,
            out_specs=whole,
            scratch_shapes=[
                vmem((2, 2 * L, half), BF16),
                vmem((2, 2 * L, half), BF16),
                vmem((2, half, 2 * L), BF16),
                vmem((2, 1, L), F32),
                vmem((nz, CAP, 2 * L), F32),
                vmem((nz, CAP, 2 * L), F32),
                vmem((nx, 2, rows, L), BF16),
                vmem((nx, rows, L), BF16),
                vmem((ny, 2, 2 * L), F32),
                vmem((ny, 2, 2 * L), F32),
                vmem((2, L), F32),
                vmem((ny, 2, L), F32),
                vmem((ny, 2, all_rows, L), BF16),
                vmem((ny, 2, all_rows, L), BF16),
                vmem((ny, all_rows, L), BF16),
                vmem((nx, 2, rows, L), BF16),
                vmem((nx, 2, rows, L), BF16),
                vmem((nz, CAP, L), F32),
                vmem((nz, CAP, L), F32),
                dma((3,)),
                dma((5,)),
                dma((5,)),
                dma((nz,)),
                dma((nz,)),
                dma((nx,)),
                dma((nx,)),
                dma((2 * nx,)),
                dma((2 * nx,)),
                dma((ny,)),
                dma((ny,)),
                dma((ny,)),
                dma((ny,)),
                dma((ny,)),
                dma((ny,)),
                dma((ny,)),
                dma((ny,)),
                dma((2 * nx,)),
                dma((2 * nx,)),
                dma((nz,)),
                dma((nz,)),
            ],
            compiler_params=pltpu.CompilerParams(collective_id=0, has_side_effects=True),
        )(tokens, gain.reshape(1, -1), bias.reshape(1, -1), group_pick, member_pick, probs, gate, up, down)

    return jax.shard_map(
        on_device,
        mesh=mesh,
        in_specs=(
            P("ep", "tp"),
            P("tp"),
            P("tp"),
            P("ep", None),
            P("ep", None),
            P("ep", None),
            P("ep", "tp", None),
            P("ep", "tp", None),
            P("ep", None, "tp"),
        ),
        out_specs=P("ep", "tp"),
        check_vma=False,
    )
```

time: 203 us -> 51.8 us (0.26)
  waiting for transfers between devices: 123 us -> 0 us
  Pallas kernels: 0 us -> 47.6 us
  blocking collectives: 46.5 us -> 0 us
  between operations: 13.5 us -> 0.01 us
  starting transfers between devices: 8.95 us -> 0 us
  matrix products: 3.75 us -> 0 us
  other arithmetic: 2.62 us -> 0 us
    psum x2 -> x0, waiting for transfers between devices: 114 us -> none  [one_axis_at_a_time(): return functools.reduce(lax.psum, axes, x)]
    pallas_call x0 -> x1, Pallas kernels: none -> 47.6 us  [on_device(): pl.pallas_call(functools.partial(kernel, nz, nx, ny, width * 2 * ny), out...]
    psum x1 -> x0, blocking collectives: 29.8 us -> none  [together(): subtotal = lax.psum(jnp.concatenate([a.ravel() for a in arrays]), axis)]
    all_to_all x1 -> x0, blocking collectives: 16.6 us -> none  [on_device(): lax.all_to_all(outgoing, 'ep', split_axis=0, concat_axis=0, tiled=True)]
    all_to_all x1 -> x0, starting transfers between devices: 8.9 us -> none  [on_device(): lax.all_to_all(by_source(results, peers, capacity), 'ep', split_axis=0, c...]
    all_to_all x1 -> x0, waiting for transfers between devices: 8.62 us -> none  [on_device(): lax.all_to_all(by_source(results, peers, capacity), 'ep', split_axis=0, c...]
    dot_general x4 -> x0, matrix products: 3.75 us -> none  [the longest x1 1.48 us: project_down(): jnp.einsum('jrf,jfd->jrd', hidden, down_weight, preferred_element_type=jn...]
    unnamed x17 -> x10, local copies, waits for them, and re-layouts: 1.42 us -> 3.95 us
  transfers between devices with their start and end apart: 3 -> 0, of which waited for: 3 -> 0; matrix products, arithmetic and copies ran while one was open for 1% -> 0% of each run, Pallas kernels for 0% -> 0%
where the time goes in v1:
time: 51.8 us; the launch traced here: 51.6 us
  Pallas kernels  47.6 us (92%)
  local copies, waits for them, and re-layouts  3.95 us (8%)
    pallas_call x1, Pallas kernels, on_device(): pl.pallas_call(functools.partial(kernel, nz, nx, ny, width * 2 * ny), out...  47.6 us
    unnamed x10, local copies, waits for them, and re-layouts  3.95 us

profile of v1, /device:TPU:1, one launch (start us, length us, event | category | flops | bytes accessed | tf_op | source)
XLA Modules:
  0.0 51.6 jit_solution(12982696977497249852)
XLA Ops:
  0.0 0.0 copy-start.2
  0.0 0.7 %copy-done.2 = s32[8,1]{0,1:T(1,128)S(1)} copy-done((s32[8,1]{0,1:T(1,128)S(1)}, s32[8,1]{0,1:T(1,128)}, u32[]{:S(2)}) %copy-start.2) | copy-done | bytes 56
  0.7 0.0 copy-start
  0.7 0.7 %copy.10.gp_ref = s32[8,1]{1,0:T(8,128)} copy(s32[8,1]{0,1:T(1,128)S(1)} %copy-done.2) | data formatting | bytes 64 | tf_op args[3]
  1.3 0.0 copy-done
  1.3 0.0 copy-start.1
  1.3 0.7 %copy.11.mp_ref = s32[8,4]{1,0:T(8,128)} copy(s32[8,4]{0,1:T(4,128)S(1)} %copy-done) | data formatting | bytes 256 | tf_op args[4]
  2.0 0.0 copy-done.1
  2.0 0.7 %copy.12.pp_ref = f32[8,4]{1,0:T(8,128)} copy(f32[8,4]{0,1:T(4,128)S(1)} %copy-done.1) | data formatting | bytes 256 | tf_op args[5]
  2.7 47.6 %shard_map.91 = bf16[8,128]{1,0:T(8,128)(2,1)} custom-call(bf16[8,128]{1,0:T(8,128)(2,1)} %tok_ref.1, f32[1,128]{1,0:T(1,128)} %bitcast.2, f32[1,128]{1,0:T(1,128)} %bitcast.3, s32[8,1]{1,0:T(8,128)} %copy.10.gp_ref, s32[8,4]{1,0:T(8,128)} %copy.11.mp_ref, f32[8,4]{1,0:T(8,128)} %copy.12.pp_ref, bf16[2,128,1024]{2,1,0:T(8,128)(2,1)} %gate_ref.1, ...), custom_call_target="tpu_custom_call" | custom-call | tf_op jit(solution)/shard_map/pallas_call | solution.py:315
  50.3 1.3 %copy.14 = bf16[8,128]{1,0:T(8,128)(2,1)} copy(bf16[8,128]{1,0:T(8,128)(2,1)} %shard_map.91) | data formatting | bytes 4096
Async XLA Ops:
  0.0 0.7 %copy-start.2 = (s32[8,1]{0,1:T(1,128)S(1)}, s32[8,1]{0,1:T(1,128)}, u32[]{:S(2)}) copy-start(s32[8,1]{0,1:T(1,128)} %param.12) | copy-start | bytes 100
  0.7 0.7 %copy-start = (s32[8,4]{0,1:T(4,128)S(1)}, s32[8,4]{0,1:T(4,128)}, u32[]{:S(2)}) copy-start(s32[8,4]{0,1:T(4,128)} %param.13) | copy-start | bytes 388
  1.3 0.7 %copy-start.1 = (f32[8,4]{0,1:T(4,128)S(1)}, f32[8,4]{0,1:T(4,128)}, u32[]{:S(2)}) copy-start(f32[8,4]{0,1:T(4,128)} %param.14) | copy-start | bytes 388

commit v2 on v1

--- a/solution.py
+++ b/solution.py
@@ -26,8 +26,9 @@
 
 def kernel(
     nz, nx, ny, features,
-    tok_ref, gain_ref, bias_ref, gp_ref, mp_ref, pp_ref, gate_ref, up_ref, down_ref,
+    tok_hbm, gain_hbm, bias_hbm, gp_hbm, mp_hbm, pp_hbm, gate_ref, up_ref, down_ref,
     out_ref,
+    tok_ref, gain_ref, bias_ref, gp_ref, mp_ref, pp_ref, isem,
     wg, wu, wd, gb,
     s1, r1, r2t, r2s, ax1s, ax1r, ax2s, ax2r, ps, pr, hb, o5s, r5, s6, r6,
     lsem, xsem_s, xsem_r, s1s, s1r, s2s_s, s2s_r, s2t_s, s2t_r, a1s, a1r, a2s, a2r,
@@ -54,6 +55,22 @@
     def each(n, body):
         lax.fori_loop(1, n, lambda d, carry: (body(d), carry)[1], 0)
 
+    inputs = [
+        pltpu.make_async_copy(src, dst, isem.at[i])
+        for i, (src, dst) in enumerate(
+            (
+                (tok_hbm, tok_ref),
+                (gp_hbm, gp_ref),
+                (mp_hbm, mp_ref),
+                (pp_hbm, pp_ref),
+                (gain_hbm, gain_ref),
+                (bias_hbm, bias_ref),
+            )
+        )
+    ]
+    for copy in inputs:
+        copy.start()
+
     mine = pl.ds(pl.multiple_of(c * half, half), half)
     other = pl.ds(pl.multiple_of((1 - c) * half, half), half)
     local = [
@@ -73,25 +90,32 @@
     each(ny, lambda d: greet(dy=d))
     each(2 * nx, lambda k: greet(dx=k // 2, dc=k % 2))
 
+    for copy in inputs:
+        copy.wait()
+
     group = (gp_ref[...] - z + nz) % nz
-    lane = iota((tokens, L), 1)
-    member = (group == lane // CAP).astype(F32)
-    count = jnp.zeros((tokens, L), F32)
-    sub = iota((tokens, L), 0)
+    row = iota((rows, tokens), 0)
+    lane = iota((rows, tokens), 1)
+    member = (group == row // CAP).astype(F32)
+    count = jnp.zeros((rows, tokens), F32)
     for t in range(tokens - 1):
-        count = count + jnp.where(sub > t, member[t : t + 1, :], 0.0)
-    chosen = member * (count == (lane % CAP).astype(F32)).astype(F32)
+        count = count + jnp.where(lane > t, member[:, t : t + 1], 0.0)
+    rowwise = member * (count == (row % CAP).astype(F32)).astype(F32)
     probs = pp_ref[...]
-    share = probs / jnp.sum(probs, axis=1, keepdims=True)
-    high = share.astype(BF16).astype(F32)
-    low = share - high
-    picks = mp_ref[...]
+    share = probs / jnp.sum(probs, axis=0, keepdims=True)
+    top = probs.shape[0]
+    table = [share[k : k + 1] for k in range(top)] + [mp_ref[k : k + 1].astype(F32) for k in range(top)]
+    wide = jnp.concatenate([jnp.concatenate(table + [rowwise], axis=0), jnp.zeros((2 * top + rows, L - tokens), F32)], axis=1)
+    turned = jnp.transpose(wide)[0:tokens, :]
+    chosen = turned[:, 2 * top :]
+    lane = iota((tokens, L), 1).astype(F32)
     shares = jnp.zeros((tokens, L), F32)
-    for k in range(picks.shape[1]):
-        pick = picks[:, k : k + 1]
-        shares = shares + jnp.where(lane == pick, high[:, k : k + 1], 0.0)
-        shares = shares + jnp.where(lane == pick + EPG, low[:, k : k + 1], 0.0)
-    rowwise = jnp.transpose(chosen)[0:rows, :]
+    for k in range(top):
+        high = turned[:, k : k + 1].astype(BF16).astype(F32)
+        low = turned[:, k : k + 1] - high
+        pick = turned[:, top + k : top + k + 1]
+        shares = shares + jnp.where(lane == pick, high, 0.0)
+        shares = shares + jnp.where(lane == pick + EPG, low, 0.0)
     both = jnp.concatenate([tok_ref[...].astype(F32), shares], axis=1)
     packed = jnp.zeros((rows, 2 * L), F32)
     for t in range(tokens):
@@ -314,10 +338,17 @@
         away = pl.BlockSpec(memory_space=pl.ANY)
         return pl.pallas_call(
             functools.partial(kernel, nz, nx, ny, width * 2 * ny),
-            out_shape=jax.ShapeDtypeStruct(tokens.shape, BF16),
-            in_specs=[whole] * 6 + [away] * 3,
+            out_shape=pltpu.VMEM(tokens.shape, BF16),
+            in_specs=[away] * 9,
             out_specs=whole,
             scratch_shapes=[
+                vmem(tokens.shape, BF16),
+                vmem((1, L), F32),
+                vmem((1, L), F32),
+                vmem((1, tokens.shape[0]), jnp.int32),
+                vmem(member_pick.shape[::-1], jnp.int32),
+                vmem(probs.shape[::-1], F32),
+                dma((6,)),
                 vmem((2, 2 * L, half), BF16),
                 vmem((2, 2 * L, half), BF16),
                 vmem((2, half, 2 * L), BF16),
@@ -360,7 +391,7 @@
                 dma((nz,)),
             ],
             compiler_params=pltpu.CompilerParams(collective_id=0, has_side_effects=True),
-        )(tokens, gain.reshape(1, -1), bias.reshape(1, -1), group_pick, member_pick, probs, gate, up, down)
+        )(tokens, gain.reshape(1, -1), bias.reshape(1, -1), group_pick.T, member_pick.T, probs.T, gate, up, down)
 
     return jax.shard_map(
         on_device,

time: 51.8 us -> 47.4 us (0.915)
  local copies, waits for them, and re-layouts: 3.95 us -> 0.58 us
  Pallas kernels: 47.6 us -> 46.7 us
    unnamed x10 -> x1, local copies, waits for them, and re-layouts: 3.95 us -> 0.58 us
    pallas_call x1, Pallas kernels: 47.6 us -> 46.7 us  [on_device(): pl.pallas_call(functools.partial(kernel, nz, nx, ny, width * 2 * ny), out...]
where the time goes in v2:
time: 47.4 us; the launch traced here: 47.3 us
  Pallas kernels  46.7 us (99%)
  local copies, waits for them, and re-layouts  0.58 us (1%)
    pallas_call x1, Pallas kernels, on_device(): pl.pallas_call(functools.partial(kernel, nz, nx, ny, width * 2 * ny), out...  46.7 us

profile of v2, /device:TPU:1, one launch (start us, length us, event | category | flops | bytes accessed | tf_op | source)
XLA Modules:
  0.0 47.3 jit_solution(16511207887618227597)
XLA Ops:
  0.0 46.7 %shard_map.91 = bf16[8,128]{1,0:T(8,128)(2,1)S(1)} custom-call(bf16[8,128]{1,0:T(8,128)(2,1)} %tok_hbm.1, f32[1,128]{1,0:T(1,128)} %bitcast.7, f32[1,128]{1,0:T(1,128)} %bitcast.8, s32[1,8]{1,0:T(1,128)} %bitcast.9, s32[4,8]{1,0:T(4,128)} %bitcast.5, f32[4,8]{1,0:T(4,128)} %bitcast.6, bf16[2,128,1024]{2,1,0:T(8,128)(2,1)} %gate_ref.1, ...), custom_call_target="tpu_custom_call" | custom-call | tf_op jit(solution)/shard_map/pallas_call | solution.py:339
  46.7 0.6 %copy.11 = bf16[8,128]{1,0:T(8,128)(2,1)} copy(bf16[8,128]{1,0:T(8,128)(2,1)S(1)} %shard_map.91) | data formatting | bytes 4096

commit v3 on v2

v3 whole, which is shorter than its diff:
```python
import functools

import jax
import jax.numpy as jnp
from jax import lax
from jax.experimental import pallas as pl
from jax.experimental.pallas import tpu as pltpu
from jax.sharding import PartitionSpec as P

EPG = 8
CAP = 2
norm_epsilon = 1e-05
MESH = pl.DeviceIdType.MESH
F32 = jnp.float32
BF16 = jnp.bfloat16
L = 128


def iota(shape, axis):
    return lax.broadcasted_iota(jnp.int32, shape, axis)


def far_first(n):
    return sorted(range(1, n), key=lambda d: -min(d, n - d))


def kernel(
    nz, nx, ny, features,
    tok_hbm, gain_hbm, bias_hbm, gp_hbm, mp_hbm, pp_hbm, gate_hbm, up_hbm, down_hbm,
    out_ref,
    tok_ref, gain_ref, bias_ref, gp_ref, mp_ref, pp_ref,
    wgu, wd, gb,
    xt, xs, zt, zs, tr, sr, ax1s, ax1r, ax2s, ax2r, ps, pr, hb, os, rr,
    zready, yin, ygo, isem, lsem, wsem, ssem, rsem, psem, hsem,
):
    tokens = tok_ref.shape[0]
    half = wgu.shape[3]
    rows = nz * CAP
    per_plane = nx * CAP
    all_rows = nz * per_plane
    per_expert = ny // 2
    ep, tp = lax.axis_index("ep"), lax.axis_index("tp")
    z, x, y, c = ep // nx, ep % nx, tp // 2, tp % 2

    def dev(dz=0, dx=0, dy=0, dc=0):
        return {
            "ep": lax.rem(z + dz + nz, nz) * nx + lax.rem(x + dx + nx, nx),
            "tp": lax.rem(y + dy + ny, ny) * 2 + lax.rem(c + dc, 2),
        }

    def remote(src, dst, ss, rs, device):
        return pltpu.make_async_remote_copy(
            src_ref=src, dst_ref=dst, send_sem=ss, recv_sem=rs, device_id=device, device_id_type=MESH
        )

    def each(n, body):
        lax.fori_loop(1, n, lambda d, carry: (body(d), carry)[1], 0)

    def done(ref, sem):
        pltpu.make_async_copy(ref, ref, sem).wait()

    def signal(sem, device):
        pl.semaphore_signal(sem, inc=1, device_id=device, device_id_type=MESH)

    barrier = pltpu.get_barrier_semaphore()
    lax.fori_loop(
        z + 1, nz, lambda to, carry: (signal(barrier, {"ep": to * nx + x, "tp": tp}), carry)[1], 0
    )
    each(2 * nx, lambda k: signal(barrier, dev(dx=k // 2, dc=k % 2)))

    @pl.when(y == 0)
    def _():
        each(ny, lambda d: signal(barrier, dev(dy=d)))

    inputs = [
        pltpu.make_async_copy(src, dst, isem.at[i])
        for i, (src, dst) in enumerate(
            (
                (gp_hbm, gp_ref),
                (mp_hbm, mp_ref),
                (pp_hbm, pp_ref),
                (tok_hbm, tok_ref),
                (gain_hbm, gain_ref),
                (bias_hbm, bias_ref),
            )
        )
    ]
    for copy in inputs:
        copy.start()

    mine = pl.ds(pl.multiple_of(c * half, half), half)
    other = pl.ds(pl.multiple_of((1 - c) * half, half), half)
    pltpu.make_async_copy(gate_hbm.at[:, :, mine], wgu.at[0, :, 0:L, :], lsem.at[0]).start()
    pltpu.make_async_copy(up_hbm.at[:, :, mine], wgu.at[1, :, 0:L, :], lsem.at[0]).start()
    pltpu.make_async_copy(down_hbm.at[:, mine, :], wd.at[:, :, 0:L], lsem.at[1]).start()

    for copy in inputs:
        copy.wait()

    group = (gp_ref[...] - z + nz) % nz
    row = iota((rows, tokens), 0)
    lane = iota((rows, tokens), 1)
    member = (group == row // CAP).astype(F32)
    count = jnp.zeros((rows, tokens), F32)
    for t in range(tokens - 1):
        count = count + jnp.where(lane > t, member[:, t : t + 1], 0.0)
    rowwise = member * (count == (row % CAP).astype(F32)).astype(F32)
    probs = pp_ref[...]
    share = probs / jnp.sum(probs, axis=0, keepdims=True)
    top = probs.shape[0]
    table = [share[k : k + 1] for k in range(top)]
    table = table + [mp_ref[k : k + 1].astype(F32) for k in range(top)] + [rowwise]
    table = jnp.concatenate(table, axis=0)
    table = jnp.concatenate([table, jnp.zeros((2 * top + rows, L - tokens), F32)], axis=1)
    turned = jnp.transpose(table)[0:tokens, :]
    chosen = turned[:, 2 * top :]
    lane = iota((tokens, L), 1).astype(F32)
    shares = jnp.zeros((tokens, L), F32)
    for k in range(top):
        high = turned[:, k : k + 1].astype(BF16).astype(F32)
        low = turned[:, k : k + 1] - high
        pick = turned[:, top + k : top + k + 1]
        shares = shares + jnp.where(lane == pick, high, 0.0)
        shares = shares + jnp.where(lane == pick + EPG, low, 0.0)
    both = jnp.concatenate([tok_ref[...].astype(F32), shares], axis=1)
    packed = jnp.zeros((rows, 2 * L), F32)
    for t in range(tokens):
        packed = packed + rowwise[:, t : t + 1] * both[t : t + 1, :]
    xt[0] = packed[:, 0:L].astype(BF16)
    xs[0] = packed[:, L : 2 * L].astype(BF16)

    pl.semaphore_wait(barrier, (2 * nx - 1) + z + jnp.where(y > 0, 1, 0))
    lax.fori_loop(0, z, lambda to, carry: (signal(zready, {"ep": to * nx + x, "tp": tp}), carry)[1], 0)

    def x_copy(k):
        return remote(xt.at[0], xt.at[k], ssem.at[0], rsem.at[0], dev(dx=k // 2, dc=k % 2))

    def x_shares(dx):
        return remote(xs.at[0], xs.at[dx], ssem.at[1], rsem.at[1], dev(dx=dx))

    each(2 * nx, lambda k: x_copy(k).start())
    each(nx, lambda k: x_shares(k).start())

    @pl.when(y > 0)
    def _():
        signal(yin, {"ep": ep, "tp": c})

    to = dev(dc=1)
    remote(gain_ref, gb.at[0], wsem.at[0], wsem.at[1], to).start()
    remote(bias_ref, gb.at[1], wsem.at[0], wsem.at[1], to).start()
    remote(gate_hbm.at[:, :, other], wgu.at[0, :, L : 2 * L, :], wsem.at[2], wsem.at[3], to).start()
    remote(up_hbm.at[:, :, other], wgu.at[1, :, L : 2 * L, :], wsem.at[2], wsem.at[3], to).start()
    remote(down_hbm.at[:, other, :], wd.at[:, :, L : 2 * L], wsem.at[4], wsem.at[5], to).start()

    done(xt.at[pl.ds(1, 2 * nx - 1)], rsem.at[0])

    for dc in range(2):
        parts = [xt[2 * dx + dc].astype(F32) for dx in range(nx)]
        for d in range(nz):
            block = [part[d * CAP : (d + 1) * CAP, :] for part in parts]
            zt[d, :, dc * L : (dc + 1) * L] = jnp.concatenate(block, axis=0).astype(BF16)
    tr[0] = zt[0]

    @pl.when(z < nz - 1)
    def _():
        pl.semaphore_wait(zready, nz - 1 - z)


    def z_copy(d):
        return remote(zt.at[d], tr.at[d], ssem.at[2], rsem.at[2], dev(dz=d))

    def z_shares(d):
        return remote(zs.at[d], sr.at[d], ssem.at[3], rsem.at[3], dev(dz=d))

    for d in far_first(nz):
        z_copy(d).start()
    done(xs.at[pl.ds(1, nx - 1)], rsem.at[1])
    parts = [xs[dx].astype(F32) for dx in range(nx)]
    for d in range(nz):
        block = [part[d * CAP : (d + 1) * CAP, :] for part in parts]
        zs[d] = jnp.concatenate(block, axis=0).astype(BF16)
    sr[0] = zs[0]
    each(nz, lambda d: z_shares(d).start())

    @pl.when(y == 0)
    def _():
        pl.semaphore_wait(yin, ny - 1)
        each(ny, lambda d: signal(ygo, dev(dy=d)))

    done(wgu.at[:, :, 0:L, :], lsem.at[0])
    done(gb, wsem.at[1])
    done(wgu.at[:, :, L : 2 * L, :], wsem.at[3])
    gain = jnp.concatenate([gain_ref[...], gb[0]], axis=1)
    bias = jnp.concatenate([bias_ref[...], gb[1]], axis=1)
    gain_high = gain.astype(BF16).astype(F32)
    bias_high = bias.astype(BF16).astype(F32)
    four = iota((16, 2 * L), 0)
    vectors = jnp.where(four == 0, gain_high, 0.0) + jnp.where(four == 1, gain - gain_high, 0.0)
    vectors = vectors + jnp.where(four == 2, bias_high, 0.0) + jnp.where(four == 3, bias - bias_high, 0.0)
    vectors = vectors.astype(BF16)
    for e in range(2):
        for side in range(2):
            line = jnp.dot(vectors, wgu[side, e], preferred_element_type=F32)
            for j in range(per_expert):
                part = line[:, j * L : (j + 1) * L]
                ax1s[e * per_expert + j, 0:1, side * L : (side + 1) * L] = part[0:1] + part[1:2]
                ax1s[e * per_expert + j, 1:2, side * L : (side + 1) * L] = part[2:3] + part[3:4]
    ax1r[0] = ax1s[y]

    @pl.when(y > 0)
    def _():
        pl.semaphore_wait(ygo, 1)

    def a1_copy(d):
        return remote(ax1s.at[(y + d) % ny], ax1r.at[d], ssem.at[4], rsem.at[4], dev(dy=d))

    each(ny, lambda d: a1_copy(d).start())

    done(tr.at[pl.ds(1, nz - 1)], rsem.at[2])

    values = jnp.concatenate([tr[d].astype(F32) for d in range(nz)], axis=0)
    middle = jnp.sum(values, axis=1, keepdims=True) * (1.0 / (2 * L))
    values = values - middle
    scaled = (values * gain).astype(BF16)

    def p_copy(d):
        return remote(ps.at[d - 1], pr.at[d - 1], ssem.at[6], psem.at[d - 1], dev(dy=d))

    def a2_copy(d):
        return remote(ax2s.at[0], ax2r.at[d], ssem.at[5], rsem.at[5], dev(dy=d))

    gate_own = up_own = None
    for place, d in enumerate(far_first(ny) + [0]):
        q = (y + d) % ny
        e = q // per_expert
        cols = pl.ds(pl.multiple_of((q % per_expert) * L, L), L)
        gate_part = jnp.dot(scaled, wgu[0, e, :, cols], preferred_element_type=F32)
        up_part = jnp.dot(scaled, wgu[1, e, :, cols], preferred_element_type=F32)
        if d == 0:
            gate_own, up_own = gate_part, up_part
        else:
            ps[d - 1, 0] = gate_part.astype(BF16)
            ps[d - 1, 1] = up_part.astype(BF16)
            p_copy(d).start()
        if place == min(2, ny - 2):
            squares = jnp.sum(values * values, axis=1, keepdims=True)
            lanes = iota((all_rows, L), 1)
            columns = jnp.where(lanes == 0, middle, 0.0) + jnp.where(lanes == 1, squares, 0.0)
            columns = jnp.transpose(columns)
            ax2s[0, :, 0:all_rows] = columns[0:2, :]
            ax2r[0, :, 0:all_rows] = columns[0:2, :]
            each(ny, lambda d: a2_copy(d).start())

    done(sr.at[pl.ds(1, nz - 1)], rsem.at[3])
    expert = 2 * x + y // per_expert
    lanes = iota((all_rows, L), 1)
    share = jnp.concatenate([sr[d].astype(F32) for d in range(nz)], axis=0)
    share = jnp.sum(
        jnp.where((lanes == expert) | (lanes == expert + EPG), share, 0.0), axis=1, keepdims=True
    )
    done(ax1r.at[pl.ds(1, ny - 1)], rsem.at[4])
    done(ax2r.at[pl.ds(1, ny - 1)], rsem.at[5])
    means = [ax2r[d, 0:1, 0:all_rows] for d in range(ny)]
    center = sum(means) * (1.0 / ny)
    shifts = [m - center for m in means]
    spread = sum(ax2r[d, 1:2, 0:all_rows] for d in range(ny)) + (features // ny) * sum(s * s for s in shifts)
    scale = lax.rsqrt(spread * (1.0 / features) + norm_epsilon)
    stack = iota((16, all_rows), 0)
    table = jnp.where(stack == ny, scale, 0.0)
    for d in range(ny):
        table = table + jnp.where(stack == d, shifts[d], 0.0)
    table = jnp.transpose(table)
    scale = table[:, ny : ny + 1]
    gate, up = gate_own, up_own
    gate_bias = up_bias = jnp.zeros((1, L), F32)
    for d in range(ny):
        shift = table[:, d : d + 1]
        gate = gate + shift * ax1r[d, 0:1, 0:L]
        up = up + shift * ax1r[d, 0:1, L : 2 * L]
        gate_bias = gate_bias + ax1r[d, 1:2, 0:L]
        up_bias = up_bias + ax1r[d, 1:2, L : 2 * L]

    for d in sorted(range(1, ny), key=lambda d: min(d, ny - d)):
        p_copy(d).wait_recv()
        gate = gate + pr[d - 1, 0].astype(F32)
        up = up + pr[d - 1, 1].astype(F32)
    gate = gate * scale + gate_bias
    up = up * scale + up_bias
    hidden = (share * (gate / (1.0 + jnp.exp(-gate)) * up)).astype(BF16)
    hb[0] = hidden

    def h_copy(d):
        return remote(hb.at[0], hb.at[d], ssem.at[7], hsem.at[d - 1], dev(dy=d))

    for d in far_first(ny):
        h_copy(d).start()

    def down(d):
        q = (y - d + ny) % ny
        units = pl.ds(pl.multiple_of((q % per_expert) * L, L), L)
        return jnp.dot(hb[d], wd[q // per_expert, units, :], preferred_element_type=F32)

    done(wd.at[:, :, 0:L], lsem.at[1])
    done(wd.at[:, :, L : 2 * L], wsem.at[5])
    total = down(0)
    for d in sorted(range(1, ny), key=lambda d: min(d, ny - d)):
        h_copy(d).wait_recv()
        total = total + down(d)

    for d in range(nz):
        for k in range(2 * nx):
            dx, dc = k // 2, k % 2
            at = d * per_plane + dx * CAP
            os[d * 2 * nx + k] = total[at : at + CAP, dc * L : (dc + 1) * L].astype(BF16)
    rr[0] = os[0]

    back_z = [lax.rem(z - d + nz, nz) * nx for d in range(nz)]
    back_x = [lax.rem(x - d + nx, nx) for d in range(nx)]
    back_tp = [tp, tp + 1 - 2 * c]
    ring = lambda d, n: min(d, n - d)
    for i in sorted(
        range(1, 2 * nx * nz), key=lambda i: -ring(i // (2 * nx), nz) - ring(i // 2 % nx, nx)
    ):
        to = {"ep": back_z[i // (2 * nx)] + back_x[i // 2 % nx], "tp": back_tp[i % 2]}
        remote(os.at[i], rr.at[i], ssem.at[8], rsem.at[6], to).start()

    done(xt.at[pl.ds(1, 2 * nx - 1)], ssem.at[0])
    done(xs.at[pl.ds(1, nx - 1)], ssem.at[1])
    done(tr.at[pl.ds(1, nz - 1)], ssem.at[2])
    done(sr.at[pl.ds(1, nz - 1)], ssem.at[3])
    done(ax1r.at[pl.ds(1, ny - 1)], ssem.at[4])
    done(ax2r.at[pl.ds(1, ny - 1)], ssem.at[5])
    done(ps, ssem.at[6])
    done(hb.at[pl.ds(1, ny - 1)], ssem.at[7])
    done(gb, wsem.at[0])
    done(wgu.at[:, :, 0:L, :], wsem.at[2])
    done(wd.at[:, :, 0:L], wsem.at[4])
    done(rr.at[pl.ds(1, 2 * nx * nz - 1)], rsem.at[6])

    result = jnp.zeros((tokens, L), F32)
    for d in range(nz):
        back = rr[d * 2 * nx].astype(F32)
        for k in range(1, 2 * nx):
            back = back + rr[d * 2 * nx + k].astype(F32)
        for s in range(CAP):
            at = d * CAP + s
            result = result + chosen[:, at : at + 1] * back[s : s + 1, :]
    out_ref[...] = result.astype(BF16)
    done(os.at[pl.ds(1, 2 * nx * nz - 1)], ssem.at[8])


def solution(mesh):
    nx = EPG // 2
    nz = mesh.shape["ep"] // nx
    ny = mesh.shape["tp"] // 2

    def on_device(tokens, gain, bias, group_pick, member_pick, probs, gate, up, down):
        width = tokens.shape[1]
        half = gate.shape[2] // 2
        rows = nz * CAP
        all_rows = nx * rows
        vmem, dma = pltpu.VMEM, pltpu.SemaphoreType.DMA
        whole = pl.BlockSpec(memory_space=pltpu.VMEM)
        away = pl.BlockSpec(memory_space=pl.ANY)
        return pl.pallas_call(
            functools.partial(kernel, nz, nx, ny, width * 2 * ny),
            out_shape=pltpu.VMEM(tokens.shape, BF16),
            in_specs=[away] * 9,
            out_specs=whole,
            scratch_shapes=[
                vmem(tokens.shape, BF16),
                vmem((1, L), F32),
                vmem((1, L), F32),
                vmem((1, tokens.shape[0]), jnp.int32),
                vmem(member_pick.shape[::-1], jnp.int32),
                vmem(probs.shape[::-1], F32),
                vmem((2, 2, 2 * L, half), BF16),
                vmem((2, half, 2 * L), BF16),
                vmem((2, 1, L), F32),
                vmem((2 * nx, rows, L), BF16),
                vmem((nx, rows, L), BF16),
                vmem((nz, nx * CAP, 2 * L), BF16),
                vmem((nz, nx * CAP, L), BF16),
                vmem((nz, nx * CAP, 2 * L), BF16),
                vmem((nz, nx * CAP, L), BF16),
                vmem((ny, 2, 2 * L), F32),
                vmem((ny, 2, 2 * L), F32),
                vmem((1, 2, L), F32),
                vmem((ny, 2, L), F32),
                vmem((ny - 1, 2, all_rows, L), BF16),
                vmem((ny - 1, 2, all_rows, L), BF16),
                vmem((ny, all_rows, L), BF16),
                vmem((2 * nx * nz, CAP, L), BF16),
                vmem((2 * nx * nz, CAP, L), BF16),
                pltpu.SemaphoreType.REGULAR,
                pltpu.SemaphoreType.REGULAR,
                pltpu.SemaphoreType.REGULAR,
                dma((6,)),
                dma((2,)),
                dma((6,)),
                dma((9,)),
                dma((7,)),
                dma((ny - 1,)),
                dma((ny - 1,)),
            ],
            compiler_params=pltpu.CompilerParams(collective_id=0, has_side_effects=True),
        )(tokens, gain.reshape(1, -1), bias.reshape(1, -1), group_pick.T, member_pick.T, probs.T, gate, up, down)

    return jax.shard_map(
        on_device,
        mesh=mesh,
        in_specs=(
            P("ep", "tp"),
            P("tp"),
            P("tp"),
            P("ep", None),
            P("ep", None),
            P("ep", None),
            P("ep", "tp", None),
            P("ep", "tp", None),
            P("ep", None, "tp"),
        ),
        out_specs=P("ep", "tp"),
        check_vma=False,
    )
```

time: 47.4 us -> 42.2 us (0.89)
  Pallas kernels: 46.7 us -> 41.5 us
    pallas_call x1, Pallas kernels: 46.7 us -> 41.5 us  [on_device(): pl.pallas_call(functools.partial(kernel, nz, nx, ny, width * 2 * ny), out...]
where the time goes in v3:
time: 42.2 us; the launch traced here: 42.1 us
  Pallas kernels  41.5 us (98%)
  local copies, waits for them, and re-layouts  0.58 us (1%)
    pallas_call x1, Pallas kernels, on_device(): pl.pallas_call(functools.partial(kernel, nz, nx, ny, width * 2 * ny), out...  41.5 us

profile of v3, /device:TPU:1, one launch (start us, length us, event | category | flops | bytes accessed | tf_op | source)
XLA Modules:
  0.0 42.1 jit_solution(6574570790750734512)
XLA Ops:
  0.0 41.5 %shard_map.91 = bf16[8,128]{1,0:T(8,128)(2,1)S(1)} custom-call(bf16[8,128]{1,0:T(8,128)(2,1)} %tok_hbm.1, f32[1,128]{1,0:T(1,128)} %bitcast.7, f32[1,128]{1,0:T(1,128)} %bitcast.8, s32[1,8]{1,0:T(1,128)} %bitcast.9, s32[4,8]{1,0:T(4,128)} %bitcast.5, f32[4,8]{1,0:T(4,128)} %bitcast.6, bf16[2,128,1024]{2,1,0:T(8,128)(2,1)} %gate_hbm.1, ...), custom_call_target="tpu_custom_call" | custom-call | tf_op jit(solution)/shard_map/pallas_call | solution.py:365
  41.5 0.6 %copy.11 = bf16[8,128]{1,0:T(8,128)(2,1)} copy(bf16[8,128]{1,0:T(8,128)(2,1)S(1)} %shard_map.91) | data formatting | bytes 4096

commit v4 on v3

v4 whole, which is shorter than its diff:
```python
import functools

import jax
import jax.numpy as jnp
from jax import lax
from jax.experimental import pallas as pl
from jax.experimental.pallas import tpu as pltpu
from jax.sharding import PartitionSpec as P

EPG = 8
CAP = 2
norm_epsilon = 1e-05
MESH = pl.DeviceIdType.MESH
F32 = jnp.float32
BF16 = jnp.bfloat16
L = 128


def iota(shape, axis):
    return lax.broadcasted_iota(jnp.int32, shape, axis)


def far_first(n):
    return sorted(range(1, n), key=lambda d: -min(d, n - d))


def kernel(
    nz, nx, ny, features,
    tok_hbm, gain_hbm, bias_hbm, gp_hbm, mp_hbm, pp_hbm, gate_hbm, up_hbm, down_hbm,
    out_ref,
    tok_ref, gain_ref, bias_ref, gp_ref, mp_ref, pp_ref,
    wgu, wd, gb,
    xt, xs, zs, tr, sr, ax1s, ax1r, ax2s, ax2r, ps, pr, hb, os, rr,
    zready, yready, isem, lsem, wsem, ssem, rsem, tsem, asem, psem, hsem,
):
    tokens = tok_ref.shape[0]
    half = wgu.shape[3]
    rows = nz * CAP
    per_plane = nx * CAP
    all_rows = nz * per_plane
    per_expert = ny // 2
    ep, tp = lax.axis_index("ep"), lax.axis_index("tp")
    z, x, y, c = ep // nx, ep % nx, tp // 2, tp % 2

    def dev(dz=0, dx=0, dy=0, dc=0):
        return {
            "ep": lax.rem(z + dz + nz, nz) * nx + lax.rem(x + dx + nx, nx),
            "tp": lax.rem(y + dy + ny, ny) * 2 + lax.rem(c + dc, 2),
        }

    def remote(src, dst, ss, rs, device):
        return pltpu.make_async_remote_copy(
            src_ref=src, dst_ref=dst, send_sem=ss, recv_sem=rs, device_id=device, device_id_type=MESH
        )

    def each(n, body):
        lax.fori_loop(1, n, lambda d, carry: (body(d), carry)[1], 0)

    def done(ref, sem):
        pltpu.make_async_copy(ref, ref, sem).wait()

    def signal(sem, device):
        pl.semaphore_signal(sem, inc=1, device_id=device, device_id_type=MESH)

    inputs = [
        pltpu.make_async_copy(src, dst, isem.at[i])
        for i, (src, dst) in enumerate(
            (
                (gp_hbm, gp_ref),
                (mp_hbm, mp_ref),
                (pp_hbm, pp_ref),
                (tok_hbm, tok_ref),
                (gain_hbm, gain_ref),
                (bias_hbm, bias_ref),
            )
        )
    ]
    for copy in inputs:
        copy.start()

    def planes(low, high, body):
        lax.fori_loop(low, high, lambda to, carry: (body(to), carry)[1], 0)

    part = nz // 2
    side = z // part
    first = side * part

    def ranked(r):
        return r + r // per_expert * (3 * per_expert - 1 - 2 * r)

    rank = ranked(y)
    barrier = pltpu.get_barrier_semaphore()

    def greet(to):
        signal(barrier, {"ep": to * nx + x, "tp": tp})

    planes(z + 1, first + part, greet)
    each(2 * nx, lambda k: signal(barrier, dev(dx=k // 2, dc=k % 2)))

    planes(rank + 1, ny, lambda r: signal(barrier, {"ep": ep, "tp": 2 * ranked(r) + c}))

    mine = pl.ds(pl.multiple_of(c * half, half), half)
    other = pl.ds(pl.multiple_of((1 - c) * half, half), half)
    pltpu.make_async_copy(gate_hbm.at[:, :, mine], wgu.at[0, :, 0:L, :], lsem.at[0]).start()
    pltpu.make_async_copy(up_hbm.at[:, :, mine], wgu.at[1, :, 0:L, :], lsem.at[0]).start()
    pltpu.make_async_copy(down_hbm.at[:, mine, :], wd.at[:, :, 0:L], lsem.at[1]).start()

    for copy in inputs:
        copy.wait()

    group = (gp_ref[...] - z + 1 + nz) % nz
    row = iota((rows, tokens), 0)
    lane = iota((rows, tokens), 1)
    member = (group == row // CAP).astype(F32)
    count = jnp.zeros((rows, tokens), F32)
    for t in range(tokens - 1):
        count = count + jnp.where(lane > t, member[:, t : t + 1], 0.0)
    rowwise = member * (count == (row % CAP).astype(F32)).astype(F32)
    def pack(source):
        packed = jnp.zeros((rows, L), F32)
        for t in range(tokens):
            packed = packed + rowwise[:, t : t + 1] * source[t : t + 1, :]
        return packed

    packed = pack(tok_ref[...].astype(F32))
    for d in range(nz):
        xt[0, d] = packed[d * CAP : (d + 1) * CAP, :].astype(BF16)
    tr[1, 0] = packed[CAP : 2 * CAP, :].astype(BF16)

    pl.semaphore_wait(barrier, (2 * nx - 1) + z + rank)
    planes(0, z, lambda to: signal(zready.at[z], {"ep": to * nx + x, "tp": tp}))
    planes(0, rank, lambda r: signal(yready, {"ep": ep, "tp": 2 * ranked(r) + c}))

    @pl.when(side == 0)
    def _():
        planes(part, nz, greet)

    def x_copy(k):
        return remote(xt.at[0], xt.at[k], ssem.at[0], rsem.at[0], dev(dx=k // 2, dc=k % 2))

    def x_shares(dx):
        return remote(xs.at[0], xs.at[dx], ssem.at[1], rsem.at[1], dev(dx=dx))

    each(2 * nx, lambda k: x_copy(k).start())

    go_x = [lax.rem(x + d, nx) for d in range(nx)]
    go_tp = [tp, tp + 1 - 2 * c]

    def straight(to):
        i = lax.rem(to - z + 1 + nz, nz)
        for k in range(2 * nx):
            device = {"ep": to * nx + go_x[k // 2], "tp": go_tp[k % 2]}
            remote(xt.at[0, i], tr.at[i, k], ssem.at[2], tsem.at[i // part], device).start()

    @pl.when(side == 1)
    def _():
        planes(0, part, straight)

    to = dev(dc=1)
    remote(gain_ref, gb.at[0], wsem.at[0], wsem.at[1], to).start()
    remote(bias_ref, gb.at[1], wsem.at[0], wsem.at[1], to).start()
    remote(gate_hbm.at[:, :, other], wgu.at[0, :, L : 2 * L, :], wsem.at[2], wsem.at[3], to).start()
    remote(up_hbm.at[:, :, other], wgu.at[1, :, L : 2 * L, :], wsem.at[2], wsem.at[3], to).start()
    remote(down_hbm.at[:, other, :], wd.at[:, :, L : 2 * L], wsem.at[4], wsem.at[5], to).start()

    probs = pp_ref[...]
    share = probs / jnp.sum(probs, axis=0, keepdims=True)
    top = probs.shape[0]
    table = [share[k : k + 1] for k in range(top)]
    table = table + [mp_ref[k : k + 1].astype(F32) for k in range(top)] + [rowwise]
    table = jnp.concatenate(table, axis=0)
    table = jnp.concatenate([table, jnp.zeros((2 * top + rows, L - tokens), F32)], axis=1)
    turned = jnp.transpose(table)[0:tokens, :]
    chosen = turned[:, 2 * top :]
    lane = iota((tokens, L), 1).astype(F32)
    shares = jnp.zeros((tokens, L), F32)
    for k in range(top):
        high = turned[:, k : k + 1].astype(BF16).astype(F32)
        low = turned[:, k : k + 1] - high
        pick = turned[:, top + k : top + k + 1]
        shares = shares + jnp.where(lane == pick, high, 0.0)
        shares = shares + jnp.where(lane == pick + EPG, low, 0.0)
    xs[0] = pack(shares).astype(BF16)
    each(nx, lambda k: x_shares(k).start())

    done(wgu.at[:, :, 0:L, :], lsem.at[0])
    done(gb, wsem.at[1])
    done(wgu.at[:, :, L : 2 * L, :], wsem.at[3])
    gain = jnp.concatenate([gain_ref[...], gb[0]], axis=1)
    bias = jnp.concatenate([bias_ref[...], gb[1]], axis=1)
    gain_high = gain.astype(BF16).astype(F32)
    bias_high = bias.astype(BF16).astype(F32)
    four = iota((16, 2 * L), 0)
    vectors = jnp.where(four == 0, gain_high, 0.0) + jnp.where(four == 1, gain - gain_high, 0.0)
    vectors = vectors + jnp.where(four == 2, bias_high, 0.0) + jnp.where(four == 3, bias - bias_high, 0.0)
    vectors = vectors.astype(BF16)
    for e in range(2):
        for g in range(2):
            line = jnp.dot(vectors, wgu[g, e], preferred_element_type=F32)
            for j in range(per_expert):
                piece = line[:, j * L : (j + 1) * L]
                ax1s[e * per_expert + j, 0:1, g * L : (g + 1) * L] = piece[0:1] + piece[1:2]
                ax1s[e * per_expert + j, 1:2, g * L : (g + 1) * L] = piece[2:3] + piece[3:4]
    ax1r[0] = ax1s[y]

    done(xt.at[pl.ds(1, 2 * nx - 1)], rsem.at[0])

    for k in range(1, 2 * nx):
        tr[1, k] = xt[k, 1]

    def z_copy(to):
        i = lax.rem(to - z + 1 + nz, nz)
        device = {"ep": to * nx + x, "tp": tp}
        remote(xt.at[:, i], tr.at[i], ssem.at[2], tsem.at[i // part], device).start()

    def z_ready_copy(to):
        pl.semaphore_wait(zready.at[to], 1)
        z_copy(to)

    planes(first, z, z_copy)
    planes(z + 1, first + part, z_ready_copy)

    @pl.when(side == 0)
    def _():
        planes(part, nz, z_ready_copy)

    def z_shares(d):
        i = lax.rem(d + 1, nz)
        return remote(zs.at[i], sr.at[i], ssem.at[3], rsem.at[3], dev(dz=d))

    done(xs.at[pl.ds(1, nx - 1)], rsem.at[1])
    blocks = [xs[dx].astype(F32) for dx in range(nx)]
    for d in range(nz):
        block = [b[d * CAP : (d + 1) * CAP, :] for b in blocks]
        zs[d] = jnp.concatenate(block, axis=0).astype(BF16)
    sr[1] = zs[1]
    each(nz, lambda d: z_shares(d).start())

    @pl.when(rank < ny - 1)
    def _():
        pl.semaphore_wait(yready, ny - 1 - rank)

    def a1_copy(d):
        return remote(ax1s.at[(y + d) % ny], ax1r.at[d], ssem.at[4], rsem.at[4], dev(dy=d))

    each(ny, lambda d: a1_copy(d).start())

    batch_rows = all_rows // 2
    own_batch = 1 // part

    def p_copy(b, d):
        return remote(ps.at[b, d - 1], pr.at[b, d - 1], ssem.at[6], psem.at[b, d - 1], dev(dy=d))

    def a2_copy(b, d):
        return remote(ax2s.at[b], ax2r.at[b, d], ssem.at[5], asem.at[b], dev(dy=d))

    gate_own, up_own = [], []
    for b in range(2):
        here = part - 1 if b == own_batch else part
        if here:
            done(tr.at[pl.ds(b * part, here)], tsem.at[b])

        slots = range(b * part, b * part + part)
        values = [
            jnp.concatenate([tr[i, 2 * dx + dc].astype(F32) for i in slots for dx in range(nx)], axis=0)
            for dc in range(2)
        ]
        values = jnp.concatenate(values, axis=1)
        middle = jnp.sum(values, axis=1, keepdims=True) * (1.0 / (2 * L))
        values = values - middle
        scaled = (values * gain).astype(BF16)
        for place, d in enumerate(far_first(ny) + [0]):
            q = (y + d) % ny
            e = q // per_expert
            cols = pl.ds(pl.multiple_of((q % per_expert) * L, L), L)
            gate_part = jnp.dot(scaled, wgu[0, e, :, cols], preferred_element_type=F32)
            up_part = jnp.dot(scaled, wgu[1, e, :, cols], preferred_element_type=F32)
            if d == 0:
                gate_own.append(gate_part)
                up_own.append(up_part)
            else:
                ps[b, d - 1, 0] = gate_part.astype(BF16)
                ps[b, d - 1, 1] = up_part.astype(BF16)
                p_copy(b, d).start()
            if place == 0:
                squares = jnp.sum(values * values, axis=1, keepdims=True)
                lanes = iota((batch_rows, L), 1)
                columns = jnp.where(lanes == 0, middle, 0.0) + jnp.where(lanes == 1, squares, 0.0)
                columns = jnp.transpose(columns)
                ax2s[b, :, 0:batch_rows] = columns[0:2, :]
                ax2r[b, 0, :, 0:batch_rows] = columns[0:2, :]
                each(ny, lambda d: a2_copy(b, d).start())

    def h_copy(b, d):
        return remote(hb.at[b, 0], hb.at[b, d], ssem.at[7], hsem.at[b, d - 1], dev(dy=d))

    done(sr.at[pl.ds(1, nz - 1)], rsem.at[3])
    done(ax1r.at[pl.ds(1, ny - 1)], rsem.at[4])
    expert = 2 * x + y // per_expert
    lanes = iota((batch_rows, L), 1)
    gate_bias = up_bias = jnp.zeros((1, L), F32)
    for d in range(ny):
        gate_bias = gate_bias + ax1r[d, 1:2, 0:L]
        up_bias = up_bias + ax1r[d, 1:2, L : 2 * L]
    for b in range(2):
        share = jnp.concatenate([sr[i].astype(F32) for i in range(b * part, b * part + part)], axis=0)
        share = jnp.sum(
            jnp.where((lanes == expert) | (lanes == expert + EPG), share, 0.0), axis=1, keepdims=True
        )
        done(ax2r.at[b, pl.ds(1, ny - 1)], asem.at[b])
        means = [ax2r[b, d, 0:1, 0:batch_rows] for d in range(ny)]
        center = sum(means) * (1.0 / ny)
        shifts = [m - center for m in means]
        spread = sum(ax2r[b, d, 1:2, 0:batch_rows] for d in range(ny))
        spread = spread + (features // ny) * sum(s * s for s in shifts)
        scale = lax.rsqrt(spread * (1.0 / features) + norm_epsilon)
        stack = iota((16, batch_rows), 0)
        table = jnp.where(stack == ny, scale, 0.0)
        for d in range(ny):
            table = table + jnp.where(stack == d, shifts[d], 0.0)
        table = jnp.transpose(table)
        scale = table[:, ny : ny + 1]
        gate, up = gate_own[b], up_own[b]
        for d in range(ny):
            shift = table[:, d : d + 1]
            gate = gate + shift * ax1r[d, 0:1, 0:L]
            up = up + shift * ax1r[d, 0:1, L : 2 * L]
        for d in sorted(range(1, ny), key=lambda d: min(d, ny - d)):
            p_copy(b, d).wait_recv()
            gate = gate + pr[b, d - 1, 0].astype(F32)
            up = up + pr[b, d - 1, 1].astype(F32)
        gate = gate * scale + gate_bias
        up = up * scale + up_bias
        hb[b, 0] = (share * (gate / (1.0 + jnp.exp(-gate)) * up)).astype(BF16)
        for d in far_first(ny):
            h_copy(b, d).start()

    def down(b, d):
        q = (y - d + ny) % ny
        units = pl.ds(pl.multiple_of((q % per_expert) * L, L), L)
        return jnp.dot(hb[b, d], wd[q // per_expert, units, :], preferred_element_type=F32)

    done(wd.at[:, :, 0:L], lsem.at[1])
    done(wd.at[:, :, L : 2 * L], wsem.at[5])

    back_z = [lax.rem(z - i + 1 + nz, nz) * nx for i in range(nz)]
    back_x = [lax.rem(x - d + nx, nx) for d in range(nx)]
    back_tp = [tp, tp + 1 - 2 * c]
    mine = 2 * nx

    def ring(d, n):
        return min(d % n, n - d % n)

    for b in range(2):
        total = down(b, 0)
        for d in sorted(range(1, ny), key=lambda d: min(d, ny - d)):
            h_copy(b, d).wait_recv()
            total = total + down(b, d)
        places = range(b * part * 2 * nx, (b + 1) * part * 2 * nx)
        for i in places:
            at = (i // (2 * nx) - b * part) * per_plane + (i // 2 % nx) * CAP
            os[i] = total[at : at + CAP, (i % 2) * L : (i % 2 + 1) * L].astype(BF16)
            if i == mine:
                rr[i] = total[at : at + CAP, 0:L].astype(BF16)
        for i in sorted(places, key=lambda i: -ring(i // (2 * nx) - 1, nz) - ring(i // 2 % nx, nx)):
            if i != mine:
                to = {"ep": back_z[i // (2 * nx)] + back_x[i // 2 % nx], "tp": back_tp[i % 2]}
                remote(os.at[i], rr.at[i], ssem.at[8], rsem.at[6], to).start()

    done(xt.at[pl.ds(1, 2 * nx - 1)], ssem.at[0])
    done(xs.at[pl.ds(1, nx - 1)], ssem.at[1])
    done(tr.at[pl.ds(1, nz - 1)], ssem.at[2])
    done(sr.at[pl.ds(1, nz - 1)], ssem.at[3])
    done(ax1r.at[pl.ds(1, ny - 1)], ssem.at[4])
    done(ax2r.at[:, pl.ds(1, ny - 1)], ssem.at[5])
    done(ps, ssem.at[6])
    done(hb.at[:, pl.ds(1, ny - 1)], ssem.at[7])
    done(gb, wsem.at[0])
    done(wgu.at[:, :, 0:L, :], wsem.at[2])
    done(wd.at[:, :, 0:L], wsem.at[4])
    done(rr.at[pl.ds(1, 2 * nx * nz - 1)], rsem.at[6])

    result = jnp.zeros((tokens, L), F32)
    for d in range(nz):
        back = rr[d * 2 * nx].astype(F32)
        for k in range(1, 2 * nx):
            back = back + rr[d * 2 * nx + k].astype(F32)
        for s in range(CAP):
            at = d * CAP + s
            result = result + chosen[:, at : at + 1] * back[s : s + 1, :]
    out_ref[...] = result.astype(BF16)
    done(os.at[pl.ds(1, 2 * nx * nz - 1)], ssem.at[8])


def solution(mesh):
    nx = EPG // 2
    nz = mesh.shape["ep"] // nx
    ny = mesh.shape["tp"] // 2

    def on_device(tokens, gain, bias, group_pick, member_pick, probs, gate, up, down):
        width = tokens.shape[1]
        half = gate.shape[2] // 2
        rows = nz * CAP
        all_rows = nx * rows
        vmem, dma = pltpu.VMEM, pltpu.SemaphoreType.DMA
        whole = pl.BlockSpec(memory_space=pltpu.VMEM)
        away = pl.BlockSpec(memory_space=pl.ANY)
        return pl.pallas_call(
            functools.partial(kernel, nz, nx, ny, width * 2 * ny),
            out_shape=pltpu.VMEM(tokens.shape, BF16),
            in_specs=[away] * 9,
            out_specs=whole,
            scratch_shapes=[
                vmem(tokens.shape, BF16),
                vmem((1, L), F32),
                vmem((1, L), F32),
                vmem((1, tokens.shape[0]), jnp.int32),
                vmem(member_pick.shape[::-1], jnp.int32),
                vmem(probs.shape[::-1], F32),
                vmem((2, 2, 2 * L, half), BF16),
                vmem((2, half, 2 * L), BF16),
                vmem((2, 1, L), F32),
                vmem((2 * nx, nz, CAP, L), BF16),
                vmem((nx, rows, L), BF16),
                vmem((nz, nx * CAP, L), BF16),
                vmem((nz, 2 * nx, CAP, L), BF16),
                vmem((nz, nx * CAP, L), BF16),
                vmem((ny, 2, 2 * L), F32),
                vmem((ny, 2, 2 * L), F32),
                vmem((2, 2, L), F32),
                vmem((2, ny, 2, L), F32),
                vmem((2, ny - 1, 2, all_rows // 2, L), BF16),
                vmem((2, ny - 1, 2, all_rows // 2, L), BF16),
                vmem((2, ny, all_rows // 2, L), BF16),
                vmem((2 * nx * nz, CAP, L), BF16),
                vmem((2 * nx * nz, CAP, L), BF16),
                pltpu.SemaphoreType.REGULAR((nz,)),
                pltpu.SemaphoreType.REGULAR,
                dma((6,)),
                dma((2,)),
                dma((6,)),
                dma((9,)),
                dma((7,)),
                dma((2,)),
                dma((2,)),
                dma((2, ny - 1)),
                dma((2, ny - 1)),
            ],
            compiler_params=pltpu.CompilerParams(collective_id=0, has_side_effects=True),
        )(tokens, gain.reshape(1, -1), bias.reshape(1, -1), group_pick.T, member_pick.T, probs.T, gate, up, down)

    return jax.shard_map(
        on_device,
        mesh=mesh,
        in_specs=(
            P("ep", "tp"),
            P("tp"),
            P("tp"),
            P("ep", None),
            P("ep", None),
            P("ep", None),
            P("ep", "tp", None),
            P("ep", "tp", None),
            P("ep", None, "tp"),
        ),
        out_specs=P("ep", "tp"),
        check_vma=False,
    )
```

time: 42.2 us -> 41.4 us (0.981)
  Pallas kernels: 41.5 us -> 40.6 us
    pallas_call x1, Pallas kernels: 41.5 us -> 40.6 us  [on_device(): pl.pallas_call(functools.partial(kernel, nz, nx, ny, width * 2 * ny), out...]
where the time goes in v4:
time: 41.4 us; the launch traced here: 41.2 us
  Pallas kernels  40.6 us (98%)
  local copies, waits for them, and re-layouts  0.58 us (1%)
    pallas_call x1, Pallas kernels, on_device(): pl.pallas_call(functools.partial(kernel, nz, nx, ny, width * 2 * ny), out...  40.6 us

profile of v4, /device:TPU:1, one launch (start us, length us, event | category | flops | bytes accessed | tf_op | source)
XLA Modules:
  0.0 41.2 jit_solution(5619287380475420616)
XLA Ops:
  0.0 40.6 %shard_map.91 = bf16[8,128]{1,0:T(8,128)(2,1)S(1)} custom-call(bf16[8,128]{1,0:T(8,128)(2,1)} %tok_hbm.1, f32[1,128]{1,0:T(1,128)} %bitcast.7, f32[1,128]{1,0:T(1,128)} %bitcast.8, s32[1,8]{1,0:T(1,128)} %bitcast.9, s32[4,8]{1,0:T(4,128)} %bitcast.5, f32[4,8]{1,0:T(4,128)} %bitcast.6, bf16[2,128,1024]{2,1,0:T(8,128)(2,1)} %gate_hbm.1, ...), custom_call_target="tpu_custom_call" | custom-call | tf_op jit(solution)/shard_map/pallas_call | solution.py:408
  40.6 0.6 %copy.11 = bf16[8,128]{1,0:T(8,128)(2,1)} copy(bf16[8,128]{1,0:T(8,128)(2,1)S(1)} %shard_map.91) | data formatting | bytes 4096

commit v5 on v4

--- a/solution.py
+++ b/solution.py
@@ -218,11 +218,7 @@
         z_copy(to)
 
     planes(first, z, z_copy)
-    planes(z + 1, first + part, z_ready_copy)
-
-    @pl.when(side == 0)
-    def _():
-        planes(part, nz, z_ready_copy)
+    planes(z + 1, nz, z_ready_copy)
 
     def z_shares(d):
         i = lax.rem(d + 1, nz)
@@ -255,6 +251,8 @@
         return remote(ax2s.at[b], ax2r.at[b, d], ssem.at[5], asem.at[b], dev(dy=d))
 
     gate_own, up_own = [], []
+    far = [d for d in far_first(ny) if min(d, ny - d) > 2]
+    held = []
     for b in range(2):
         here = part - 1 if b == own_batch else part
         if here:
@@ -281,7 +279,13 @@
             else:
                 ps[b, d - 1, 0] = gate_part.astype(BF16)
                 ps[b, d - 1, 1] = up_part.astype(BF16)
-                p_copy(b, d).start()
+                if b == 1 and d not in far:
+                    while held:
+                        p_copy(0, held.pop(0)).start()
+                if b == 1 or d in far:
+                    p_copy(b, d).start()
+                else:
+                    held.append(d)
             if place == 0:
                 squares = jnp.sum(values * values, axis=1, keepdims=True)
                 lanes = iota((batch_rows, L), 1)
@@ -302,6 +306,7 @@
     for d in range(ny):
         gate_bias = gate_bias + ax1r[d, 1:2, 0:L]
         up_bias = up_bias + ax1r[d, 1:2, L : 2 * L]
+    ready = []
     for b in range(2):
         share = jnp.concatenate([sr[i].astype(F32) for i in range(b * part, b * part + part)], axis=0)
         share = jnp.sum(
@@ -325,7 +330,10 @@
             shift = table[:, d : d + 1]
             gate = gate + shift * ax1r[d, 0:1, 0:L]
             up = up + shift * ax1r[d, 0:1, L : 2 * L]
-        for d in sorted(range(1, ny), key=lambda d: min(d, ny - d)):
+        ready.append((gate, up, scale, share))
+    for b in range(2):
+        gate, up, scale, share = ready[b]
+        for d in far_first(ny):
             p_copy(b, d).wait_recv()
             gate = gate + pr[b, d - 1, 0].astype(F32)
             up = up + pr[b, d - 1, 1].astype(F32)

time: 41.4 us -> 41 us (level)
  no operation moved by 1% of the time
where the time goes in v5:
time: 41 us; the launch traced here: 40.9 us
  Pallas kernels  40.3 us (98%)
  local copies, waits for them, and re-layouts  0.58 us (1%)
    pallas_call x1, Pallas kernels, on_device(): pl.pallas_call(functools.partial(kernel, nz, nx, ny, width * 2 * ny), out...  40.3 us

profile of v5, /device:TPU:1, one launch (start us, length us, event | category | flops | bytes accessed | tf_op | source)
XLA Modules:
  0.0 40.9 jit_solution(6191115128433023808)
XLA Ops:
  0.0 40.3 %shard_map.91 = bf16[8,128]{1,0:T(8,128)(2,1)S(1)} custom-call(bf16[8,128]{1,0:T(8,128)(2,1)} %tok_hbm.1, f32[1,128]{1,0:T(1,128)} %bitcast.7, f32[1,128]{1,0:T(1,128)} %bitcast.8, s32[1,8]{1,0:T(1,128)} %bitcast.9, s32[4,8]{1,0:T(4,128)} %bitcast.5, f32[4,8]{1,0:T(4,128)} %bitcast.6, bf16[2,128,1024]{2,1,0:T(8,128)(2,1)} %gate_hbm.1, ...), custom_call_target="tpu_custom_call" | custom-call | tf_op jit(solution)/shard_map/pallas_call | solution.py:416
  40.3 0.6 %copy.11 = bf16[8,128]{1,0:T(8,128)(2,1)} copy(bf16[8,128]{1,0:T(8,128)(2,1)S(1)} %shard_map.91) | data formatting | bytes 4096

commit v6 on v5

--- a/solution.py
+++ b/solution.py
@@ -89,6 +89,13 @@
         return r + r // per_expert * (3 * per_expert - 1 - 2 * r)
 
     rank = ranked(y)
+
+    def slot(source, to):
+        near = lax.rem(to - source + 1 + nz, nz)
+        near = (source + nz - 1) // nz * (near + (lax.rem(to + 1, nz) - near + nz - 1) // nz)
+        return (1 - to // part) * source + to // part * near
+
+    own_slot = slot(z, z)
     barrier = pltpu.get_barrier_semaphore()
 
     def greet(to):
@@ -125,7 +132,6 @@
     packed = pack(tok_ref[...].astype(F32))
     for d in range(nz):
         xt[0, d] = packed[d * CAP : (d + 1) * CAP, :].astype(BF16)
-    tr[1, 0] = packed[CAP : 2 * CAP, :].astype(BF16)
 
     pl.semaphore_wait(barrier, (2 * nx - 1) + z + rank)
     planes(0, z, lambda to: signal(zready.at[z], {"ep": to * nx + x, "tp": tp}))
@@ -148,9 +154,10 @@
 
     def straight(to):
         i = lax.rem(to - z + 1 + nz, nz)
+        at = slot(z, to)
         for k in range(2 * nx):
             device = {"ep": to * nx + go_x[k // 2], "tp": go_tp[k % 2]}
-            remote(xt.at[0, i], tr.at[i, k], ssem.at[2], tsem.at[i // part], device).start()
+            remote(xt.at[0, i], tr.at[at, k], ssem.at[2], tsem.at[at // part], device).start()
 
     @pl.when(side == 1)
     def _():
@@ -205,13 +212,14 @@
 
     done(xt.at[pl.ds(1, 2 * nx - 1)], rsem.at[0])
 
-    for k in range(1, 2 * nx):
-        tr[1, k] = xt[k, 1]
+    for k in range(2 * nx):
+        tr[own_slot, k] = xt[k, 1]
 
     def z_copy(to):
         i = lax.rem(to - z + 1 + nz, nz)
         device = {"ep": to * nx + x, "tp": tp}
-        remote(xt.at[:, i], tr.at[i], ssem.at[2], tsem.at[i // part], device).start()
+        at = slot(z, to)
+        remote(xt.at[:, i], tr.at[at], ssem.at[2], tsem.at[at // part], device).start()
 
     def z_ready_copy(to):
         pl.semaphore_wait(zready.at[to], 1)
@@ -222,14 +230,15 @@
 
     def z_shares(d):
         i = lax.rem(d + 1, nz)
-        return remote(zs.at[i], sr.at[i], ssem.at[3], rsem.at[3], dev(dz=d))
+        at = slot(z, lax.rem(z + d, nz))
+        return remote(zs.at[i], sr.at[at], ssem.at[3], rsem.at[3], dev(dz=d))
 
     done(xs.at[pl.ds(1, nx - 1)], rsem.at[1])
     blocks = [xs[dx].astype(F32) for dx in range(nx)]
     for d in range(nz):
         block = [b[d * CAP : (d + 1) * CAP, :] for b in blocks]
         zs[d] = jnp.concatenate(block, axis=0).astype(BF16)
-    sr[1] = zs[1]
+    sr[own_slot] = zs[1]
     each(nz, lambda d: z_shares(d).start())
 
     @pl.when(rank < ny - 1)
@@ -242,7 +251,7 @@
     each(ny, lambda d: a1_copy(d).start())
 
     batch_rows = all_rows // 2
-    own_batch = 1 // part
+    own_batch = 0
 
     def p_copy(b, d):
         return remote(ps.at[b, d - 1], pr.at[b, d - 1], ssem.at[6], psem.at[b, d - 1], dev(dy=d))
@@ -351,29 +360,41 @@
     done(wd.at[:, :, 0:L], lsem.at[1])
     done(wd.at[:, :, L : 2 * L], wsem.at[5])
 
-    back_z = [lax.rem(z - i + 1 + nz, nz) * nx for i in range(nz)]
+    back_z, back_at = [], []
+    last = lax.rem(z + 1, nz)
+    for h in range(nz):
+        source = lax.rem(z + 1 - h + (last - h + nz) // nz + nz, nz) * side if h else 0
+        source = source + (1 - side) * h
+        back_z.append(source * nx)
+        back_at.append(lax.rem(z - source + 1 + nz, nz) * 2 * nx)
     back_x = [lax.rem(x - d + nx, nx) for d in range(nx)]
     back_tp = [tp, tp + 1 - 2 * c]
-    mine = 2 * nx
-
-    def ring(d, n):
-        return min(d % n, n - d % n)
+    order = sorted(range(2 * nx), key=lambda k: -min(k // 2, nx - k // 2))
+
+    def send_back(h, k):
+        to = {"ep": back_z[h] + back_x[k // 2], "tp": back_tp[k % 2]}
+        remote(os.at[h * 2 * nx + k], rr.at[back_at[h] + k], ssem.at[8], rsem.at[6], to).start()
 
     for b in range(2):
         total = down(b, 0)
         for d in sorted(range(1, ny), key=lambda d: min(d, ny - d)):
             h_copy(b, d).wait_recv()
             total = total + down(b, d)
-        places = range(b * part * 2 * nx, (b + 1) * part * 2 * nx)
-        for i in places:
-            at = (i // (2 * nx) - b * part) * per_plane + (i // 2 % nx) * CAP
-            os[i] = total[at : at + CAP, (i % 2) * L : (i % 2 + 1) * L].astype(BF16)
-            if i == mine:
-                rr[i] = total[at : at + CAP, 0:L].astype(BF16)
-        for i in sorted(places, key=lambda i: -ring(i // (2 * nx) - 1, nz) - ring(i // 2 % nx, nx)):
-            if i != mine:
-                to = {"ep": back_z[i // (2 * nx)] + back_x[i // 2 % nx], "tp": back_tp[i % 2]}
-                remote(os.at[i], rr.at[i], ssem.at[8], rsem.at[6], to).start()
+        slots = range(b * part, (b + 1) * part)
+        for h in slots:
+            for k in range(2 * nx):
+                at = (h - b * part) * per_plane + k // 2 * CAP
+                piece = total[at : at + CAP, (k % 2) * L : (k % 2 + 1) * L]
+                os[h * 2 * nx + k] = piece.astype(BF16)
+        for h in slots:
+            for k in order:
+                if k:
+                    send_back(h, k)
+                elif b == own_batch:
+                    pl.when(own_slot != h)(functools.partial(send_back, h, k))
+                else:
+                    send_back(h, k)
+    rr[2 * nx] = os[own_slot * 2 * nx]
 
     done(xt.at[pl.ds(1, 2 * nx - 1)], ssem.at[0])
     done(xs.at[pl.ds(1, nx - 1)], ssem.at[1])

time: 41 us -> 40.3 us (0.983)
  Pallas kernels: 40.3 us -> 39.6 us
    pallas_call x1, Pallas kernels: 40.3 us -> 39.6 us  [on_device(): pl.pallas_call(functools.partial(kernel, nz, nx, ny, width * 2 * ny), out...]
where the time goes in v6:
time: 40.3 us; the launch traced here: 40.2 us
  Pallas kernels  39.6 us (98%)
  local copies, waits for them, and re-layouts  0.58 us (1%)
    pallas_call x1, Pallas kernels, on_device(): pl.pallas_call(functools.partial(kernel, nz, nx, ny, width * 2 * ny), out...  39.6 us

profile of v6, /device:TPU:1, one launch (start us, length us, event | category | flops | bytes accessed | tf_op | source)
XLA Modules:
  0.0 40.2 jit_solution(10850999928328457613)
XLA Ops:
  0.0 39.6 %shard_map.91 = bf16[8,128]{1,0:T(8,128)(2,1)S(1)} custom-call(bf16[8,128]{1,0:T(8,128)(2,1)} %tok_hbm.1, f32[1,128]{1,0:T(1,128)} %bitcast.7, f32[1,128]{1,0:T(1,128)} %bitcast.8, s32[1,8]{1,0:T(1,128)} %bitcast.9, s32[4,8]{1,0:T(4,128)} %bitcast.5, f32[4,8]{1,0:T(4,128)} %bitcast.6, bf16[2,128,1024]{2,1,0:T(8,128)(2,1)} %gate_hbm.1, ...), custom_call_target="tpu_custom_call" | custom-call | tf_op jit(solution)/shard_map/pallas_call | solution.py:437
  39.6 0.6 %copy.11 = bf16[8,128]{1,0:T(8,128)(2,1)} copy(bf16[8,128]{1,0:T(8,128)(2,1)S(1)} %shard_map.91) | data formatting | bytes 4096

commit v7 on v6

--- a/solution.py
+++ b/solution.py
@@ -260,8 +260,6 @@
         return remote(ax2s.at[b], ax2r.at[b, d], ssem.at[5], asem.at[b], dev(dy=d))
 
     gate_own, up_own = [], []
-    far = [d for d in far_first(ny) if min(d, ny - d) > 2]
-    held = []
     for b in range(2):
         here = part - 1 if b == own_batch else part
         if here:
@@ -288,13 +286,7 @@
             else:
                 ps[b, d - 1, 0] = gate_part.astype(BF16)
                 ps[b, d - 1, 1] = up_part.astype(BF16)
-                if b == 1 and d not in far:
-                    while held:
-                        p_copy(0, held.pop(0)).start()
-                if b == 1 or d in far:
-                    p_copy(b, d).start()
-                else:
-                    held.append(d)
+                p_copy(b, d).start()
             if place == 0:
                 squares = jnp.sum(values * values, axis=1, keepdims=True)
                 lanes = iota((batch_rows, L), 1)
@@ -315,7 +307,6 @@
     for d in range(ny):
         gate_bias = gate_bias + ax1r[d, 1:2, 0:L]
         up_bias = up_bias + ax1r[d, 1:2, L : 2 * L]
-    ready = []
     for b in range(2):
         share = jnp.concatenate([sr[i].astype(F32) for i in range(b * part, b * part + part)], axis=0)
         share = jnp.sum(
@@ -339,9 +330,6 @@
             shift = table[:, d : d + 1]
             gate = gate + shift * ax1r[d, 0:1, 0:L]
             up = up + shift * ax1r[d, 0:1, L : 2 * L]
-        ready.append((gate, up, scale, share))
-    for b in range(2):
-        gate, up, scale, share = ready[b]
         for d in far_first(ny):
             p_copy(b, d).wait_recv()
             gate = gate + pr[b, d - 1, 0].astype(F32)

time: 40.3 us -> 39.6 us (0.983)
  Pallas kernels: 39.6 us -> 38.6 us
    pallas_call x1, Pallas kernels: 39.6 us -> 38.6 us  [on_device(): pl.pallas_call(functools.partial(kernel, nz, nx, ny, width * 2 * ny), out...]
where the time goes in v7:
time: 39.6 us; the launch traced here: 39.2 us
  Pallas kernels  38.6 us (97%)
  local copies, waits for them, and re-layouts  0.58 us (1%)
    pallas_call x1, Pallas kernels, on_device(): pl.pallas_call(functools.partial(kernel, nz, nx, ny, width * 2 * ny), out...  38.6 us

profile of v7, /device:TPU:1, one launch (start us, length us, event | category | flops | bytes accessed | tf_op | source)
XLA Modules:
  0.0 39.2 jit_solution(13369896386993287788)
XLA Ops:
  0.0 38.6 %shard_map.91 = bf16[8,128]{1,0:T(8,128)(2,1)S(1)} custom-call(bf16[8,128]{1,0:T(8,128)(2,1)} %tok_hbm.1, f32[1,128]{1,0:T(1,128)} %bitcast.7, f32[1,128]{1,0:T(1,128)} %bitcast.8, s32[1,8]{1,0:T(1,128)} %bitcast.9, s32[4,8]{1,0:T(4,128)} %bitcast.5, f32[4,8]{1,0:T(4,128)} %bitcast.6, bf16[2,128,1024]{2,1,0:T(8,128)(2,1)} %gate_hbm.1, ...), custom_call_target="tpu_custom_call" | custom-call | tf_op jit(solution)/shard_map/pallas_call | solution.py:425
  38.6 0.6 %copy.11 = bf16[8,128]{1,0:T(8,128)(2,1)} copy(bf16[8,128]{1,0:T(8,128)(2,1)S(1)} %shard_map.91) | data formatting | bytes 4096

commit v8 on v7

--- a/solution.py
+++ b/solution.py
@@ -9,6 +9,7 @@
 
 EPG = 8
 CAP = 2
+EARLY = 2
 norm_epsilon = 1e-05
 MESH = pl.DeviceIdType.MESH
 F32 = jnp.float32
@@ -89,13 +90,7 @@
         return r + r // per_expert * (3 * per_expert - 1 - 2 * r)
 
     rank = ranked(y)
-
-    def slot(source, to):
-        near = lax.rem(to - source + 1 + nz, nz)
-        near = (source + nz - 1) // nz * (near + (lax.rem(to + 1, nz) - near + nz - 1) // nz)
-        return (1 - to // part) * source + to // part * near
-
-    own_slot = slot(z, z)
+    own_batch = (z + nz - EARLY) // nz
     barrier = pltpu.get_barrier_semaphore()
 
     def greet(to):
@@ -115,7 +110,7 @@
     for copy in inputs:
         copy.wait()
 
-    group = (gp_ref[...] - z + 1 + nz) % nz
+    group = gp_ref[...]
     row = iota((rows, tokens), 0)
     lane = iota((rows, tokens), 1)
     member = (group == row // CAP).astype(F32)
@@ -153,11 +148,9 @@
     go_tp = [tp, tp + 1 - 2 * c]
 
     def straight(to):
-        i = lax.rem(to - z + 1 + nz, nz)
-        at = slot(z, to)
         for k in range(2 * nx):
             device = {"ep": to * nx + go_x[k // 2], "tp": go_tp[k % 2]}
-            remote(xt.at[0, i], tr.at[at, k], ssem.at[2], tsem.at[at // part], device).start()
+            remote(xt.at[0, to], tr.at[z, k], ssem.at[2], tsem.at[own_batch], device).start()
 
     @pl.when(side == 1)
     def _():
@@ -213,13 +206,11 @@
     done(xt.at[pl.ds(1, 2 * nx - 1)], rsem.at[0])
 
     for k in range(2 * nx):
-        tr[own_slot, k] = xt[k, 1]
+        tr[z, k] = xt[k, z]
 
     def z_copy(to):
-        i = lax.rem(to - z + 1 + nz, nz)
         device = {"ep": to * nx + x, "tp": tp}
-        at = slot(z, to)
-        remote(xt.at[:, i], tr.at[at], ssem.at[2], tsem.at[at // part], device).start()
+        remote(xt.at[:, to], tr.at[z], ssem.at[2], tsem.at[own_batch], device).start()
 
     def z_ready_copy(to):
         pl.semaphore_wait(zready.at[to], 1)
@@ -229,16 +220,14 @@
     planes(z + 1, nz, z_ready_copy)
 
     def z_shares(d):
-        i = lax.rem(d + 1, nz)
-        at = slot(z, lax.rem(z + d, nz))
-        return remote(zs.at[i], sr.at[at], ssem.at[3], rsem.at[3], dev(dz=d))
+        return remote(zs.at[lax.rem(z + d, nz)], sr.at[z], ssem.at[3], rsem.at[3], dev(dz=d))
 
     done(xs.at[pl.ds(1, nx - 1)], rsem.at[1])
     blocks = [xs[dx].astype(F32) for dx in range(nx)]
     for d in range(nz):
         block = [b[d * CAP : (d + 1) * CAP, :] for b in blocks]
         zs[d] = jnp.concatenate(block, axis=0).astype(BF16)
-    sr[own_slot] = zs[1]
+    sr[z] = zs[z]
     each(nz, lambda d: z_shares(d).start())
 
     @pl.when(rank < ny - 1)
@@ -250,22 +239,34 @@
 
     each(ny, lambda d: a1_copy(d).start())
 
-    batch_rows = all_rows // 2
-    own_batch = 0
+    cuts = [0, EARLY, nz]
+
+    def rows_of(b):
+        return pl.ds(cuts[b] * per_plane, (cuts[b + 1] - cuts[b]) * per_plane)
 
     def p_copy(b, d):
-        return remote(ps.at[b, d - 1], pr.at[b, d - 1], ssem.at[6], psem.at[b, d - 1], dev(dy=d))
+        here = rows_of(b)
+        return remote(
+            ps.at[d - 1, :, here], pr.at[d - 1, :, here], ssem.at[6], psem.at[b, d - 1], dev(dy=d)
+        )
 
     def a2_copy(b, d):
         return remote(ax2s.at[b], ax2r.at[b, d], ssem.at[5], asem.at[b], dev(dy=d))
 
     gate_own, up_own = [], []
     for b in range(2):
-        here = part - 1 if b == own_batch else part
-        if here:
-            done(tr.at[pl.ds(b * part, here)], tsem.at[b])
-
-        slots = range(b * part, b * part + part)
+        slots = range(cuts[b], cuts[b + 1])
+        here = rows_of(b)
+        batch_rows = here.size
+
+        @pl.when(own_batch == b)
+        def _():
+            done(tr.at[pl.ds(1, len(slots) - 1)], tsem.at[b])
+
+        @pl.when(own_batch != b)
+        def _():
+            done(tr.at[pl.ds(0, len(slots))], tsem.at[b])
+
         values = [
             jnp.concatenate([tr[i, 2 * dx + dc].astype(F32) for i in slots for dx in range(nx)], axis=0)
             for dc in range(2)
@@ -284,8 +285,8 @@
                 gate_own.append(gate_part)
                 up_own.append(up_part)
             else:
-                ps[b, d - 1, 0] = gate_part.astype(BF16)
-                ps[b, d - 1, 1] = up_part.astype(BF16)
+                ps[d - 1, 0, here] = gate_part.astype(BF16)
+                ps[d - 1, 1, here] = up_part.astype(BF16)
                 p_copy(b, d).start()
             if place == 0:
                 squares = jnp.sum(values * values, axis=1, keepdims=True)
@@ -297,18 +298,21 @@
                 each(ny, lambda d: a2_copy(b, d).start())
 
     def h_copy(b, d):
-        return remote(hb.at[b, 0], hb.at[b, d], ssem.at[7], hsem.at[b, d - 1], dev(dy=d))
+        here = rows_of(b)
+        return remote(hb.at[0, here], hb.at[d, here], ssem.at[7], hsem.at[b, d - 1], dev(dy=d))
 
     done(sr.at[pl.ds(1, nz - 1)], rsem.at[3])
     done(ax1r.at[pl.ds(1, ny - 1)], rsem.at[4])
     expert = 2 * x + y // per_expert
-    lanes = iota((batch_rows, L), 1)
     gate_bias = up_bias = jnp.zeros((1, L), F32)
     for d in range(ny):
         gate_bias = gate_bias + ax1r[d, 1:2, 0:L]
         up_bias = up_bias + ax1r[d, 1:2, L : 2 * L]
     for b in range(2):
-        share = jnp.concatenate([sr[i].astype(F32) for i in range(b * part, b * part + part)], axis=0)
+        here = rows_of(b)
+        batch_rows = here.size
+        lanes = iota((batch_rows, L), 1)
+        share = jnp.concatenate([sr[i].astype(F32) for i in range(cuts[b], cuts[b + 1])], axis=0)
         share = jnp.sum(
             jnp.where((lanes == expert) | (lanes == expert + EPG), share, 0.0), axis=1, keepdims=True
         )
@@ -332,57 +336,48 @@
             up = up + shift * ax1r[d, 0:1, L : 2 * L]
         for d in far_first(ny):
             p_copy(b, d).wait_recv()
-            gate = gate + pr[b, d - 1, 0].astype(F32)
-            up = up + pr[b, d - 1, 1].astype(F32)
+            gate = gate + pr[d - 1, 0, here].astype(F32)
+            up = up + pr[d - 1, 1, here].astype(F32)
         gate = gate * scale + gate_bias
         up = up * scale + up_bias
-        hb[b, 0] = (share * (gate / (1.0 + jnp.exp(-gate)) * up)).astype(BF16)
+        hb[0, here] = (share * (gate / (1.0 + jnp.exp(-gate)) * up)).astype(BF16)
         for d in far_first(ny):
             h_copy(b, d).start()
 
     def down(b, d):
         q = (y - d + ny) % ny
         units = pl.ds(pl.multiple_of((q % per_expert) * L, L), L)
-        return jnp.dot(hb[b, d], wd[q // per_expert, units, :], preferred_element_type=F32)
+        return jnp.dot(hb[d, rows_of(b)], wd[q // per_expert, units, :], preferred_element_type=F32)
 
     done(wd.at[:, :, 0:L], lsem.at[1])
     done(wd.at[:, :, L : 2 * L], wsem.at[5])
 
-    back_z, back_at = [], []
-    last = lax.rem(z + 1, nz)
-    for h in range(nz):
-        source = lax.rem(z + 1 - h + (last - h + nz) // nz + nz, nz) * side if h else 0
-        source = source + (1 - side) * h
-        back_z.append(source * nx)
-        back_at.append(lax.rem(z - source + 1 + nz, nz) * 2 * nx)
     back_x = [lax.rem(x - d + nx, nx) for d in range(nx)]
     back_tp = [tp, tp + 1 - 2 * c]
     order = sorted(range(2 * nx), key=lambda k: -min(k // 2, nx - k // 2))
 
     def send_back(h, k):
-        to = {"ep": back_z[h] + back_x[k // 2], "tp": back_tp[k % 2]}
-        remote(os.at[h * 2 * nx + k], rr.at[back_at[h] + k], ssem.at[8], rsem.at[6], to).start()
+        to = {"ep": h * nx + back_x[k // 2], "tp": back_tp[k % 2]}
+        remote(os.at[h * 2 * nx + k], rr.at[z * 2 * nx + k], ssem.at[8], rsem.at[6], to).start()
 
     for b in range(2):
         total = down(b, 0)
         for d in sorted(range(1, ny), key=lambda d: min(d, ny - d)):
             h_copy(b, d).wait_recv()
             total = total + down(b, d)
-        slots = range(b * part, (b + 1) * part)
+        slots = range(cuts[b], cuts[b + 1])
         for h in slots:
             for k in range(2 * nx):
-                at = (h - b * part) * per_plane + k // 2 * CAP
+                at = (h - cuts[b]) * per_plane + k // 2 * CAP
                 piece = total[at : at + CAP, (k % 2) * L : (k % 2 + 1) * L]
                 os[h * 2 * nx + k] = piece.astype(BF16)
         for h in slots:
             for k in order:
                 if k:
                     send_back(h, k)
-                elif b == own_batch:
-                    pl.when(own_slot != h)(functools.partial(send_back, h, k))
                 else:
-                    send_back(h, k)
-    rr[2 * nx] = os[own_slot * 2 * nx]
+                    pl.when(z != h)(functools.partial(send_back, h, k))
+    rr[z * 2 * nx] = os[z * 2 * nx]
 
     done(xt.at[pl.ds(1, 2 * nx - 1)], ssem.at[0])
     done(xs.at[pl.ds(1, nx - 1)], ssem.at[1])
@@ -391,7 +386,7 @@
     done(ax1r.at[pl.ds(1, ny - 1)], ssem.at[4])
     done(ax2r.at[:, pl.ds(1, ny - 1)], ssem.at[5])
     done(ps, ssem.at[6])
-    done(hb.at[:, pl.ds(1, ny - 1)], ssem.at[7])
+    done(hb.at[pl.ds(1, ny - 1)], ssem.at[7])
     done(gb, wsem.at[0])
     done(wgu.at[:, :, 0:L, :], wsem.at[2])
     done(wd.at[:, :, 0:L], wsem.at[4])
@@ -446,9 +441,9 @@
                 vmem((ny, 2, 2 * L), F32),
                 vmem((2, 2, L), F32),
                 vmem((2, ny, 2, L), F32),
-                vmem((2, ny - 1, 2, all_rows // 2, L), BF16),
-                vmem((2, ny - 1, 2, all_rows // 2, L), BF16),
-                vmem((2, ny, all_rows // 2, L), BF16),
+                vmem((ny - 1, 2, all_rows, L), BF16),
+                vmem((ny - 1, 2, all_rows, L), BF16),
+                vmem((ny, all_rows, L), BF16),
                 vmem((2 * nx * nz, CAP, L), BF16),
                 vmem((2 * nx * nz, CAP, L), BF16),
                 pltpu.SemaphoreType.REGULAR((nz,)),

time: 39.6 us -> 39.7 us (level)
  the two profiles are of different devices: /device:TPU:1 before, /device:TPU:128 now
where the time goes in v8:
time: 39.7 us; the launch traced here: 39.5 us
  Pallas kernels  38.9 us (98%)
  local copies, waits for them, and re-layouts  0.58 us (1%)
    pallas_call x1, Pallas kernels, on_device(): pl.pallas_call(functools.partial(kernel, nz, nx, ny, width * 2 * ny), out...  38.9 us

profile of v8, /device:TPU:128, one launch (start us, length us, event | category | flops | bytes accessed | tf_op | source)
XLA Modules:
  0.0 39.5 jit_solution(3396032977059480157)
XLA Ops:
  0.0 38.9 %shard_map.91 = bf16[8,128]{1,0:T(8,128)(2,1)S(1)} custom-call(bf16[8,128]{1,0:T(8,128)(2,1)} %tok_hbm.1, f32[1,128]{1,0:T(1,128)} %bitcast.7, f32[1,128]{1,0:T(1,128)} %bitcast.8, s32[1,8]{1,0:T(1,128)} %bitcast.9, s32[4,8]{1,0:T(4,128)} %bitcast.5, f32[4,8]{1,0:T(4,128)} %bitcast.6, bf16[2,128,1024]{2,1,0:T(8,128)(2,1)} %gate_hbm.1, ...), custom_call_target="tpu_custom_call" | custom-call | tf_op jit(solution)/shard_map/pallas_call | solution.py:420
  39.0 0.6 %copy.11 = bf16[8,128]{1,0:T(8,128)(2,1)} copy(bf16[8,128]{1,0:T(8,128)(2,1)S(1)} %shard_map.91) | data formatting | bytes 4096

commit v9 on v8

--- a/solution.py
+++ b/solution.py
@@ -275,6 +275,7 @@
         middle = jnp.sum(values, axis=1, keepdims=True) * (1.0 / (2 * L))
         values = values - middle
         scaled = (values * gain).astype(BF16)
+        waiting = []
         for place, d in enumerate(far_first(ny) + [0]):
             q = (y + d) % ny
             e = q // per_expert
@@ -287,7 +288,18 @@
             else:
                 ps[d - 1, 0, here] = gate_part.astype(BF16)
                 ps[d - 1, 1, here] = up_part.astype(BF16)
-                p_copy(b, d).start()
+                if place == 0:
+                    p_copy(b, d).start()
+                else:
+                    waiting.append(d)
+                if place in (2, ny - 2):
+
+                    @pl.when(ep >= 0)
+                    def _():
+                        for w in waiting:
+                            p_copy(b, w).start()
+
+                    waiting = []
             if place == 0:
                 squares = jnp.sum(values * values, axis=1, keepdims=True)
                 lanes = iota((batch_rows, L), 1)
@@ -341,8 +353,12 @@
         gate = gate * scale + gate_bias
         up = up * scale + up_bias
         hb[0, here] = (share * (gate / (1.0 + jnp.exp(-gate)) * up)).astype(BF16)
-        for d in far_first(ny):
-            h_copy(b, d).start()
+
+        @pl.when(ep >= 0)
+        def _():
+            for d in far_first(ny):
+                h_copy(b, d).start()
+
 
     def down(b, d):
         q = (y - d + ny) % ny

time: 39.7 us -> 38.4 us (0.967)
  the two profiles are of different devices: /device:TPU:128 before, /device:TPU:1 now
where the time goes in v9:
time: 38.4 us; the launch traced here: 38.2 us
  Pallas kernels  37.7 us (98%)
  local copies, waits for them, and re-layouts  0.58 us (2%)
    pallas_call x1, Pallas kernels, on_device(): pl.pallas_call(functools.partial(kernel, nz, nx, ny, width * 2 * ny), out...  37.7 us

profile of v9, /device:TPU:1, one launch (start us, length us, event | category | flops | bytes accessed | tf_op | source)
XLA Modules:
  0.0 38.2 jit_solution(10675107278409929718)
XLA Ops:
  0.0 37.7 %shard_map.91 = bf16[8,128]{1,0:T(8,128)(2,1)S(1)} custom-call(bf16[8,128]{1,0:T(8,128)(2,1)} %tok_hbm.1, f32[1,128]{1,0:T(1,128)} %bitcast.7, f32[1,128]{1,0:T(1,128)} %bitcast.8, s32[1,8]{1,0:T(1,128)} %bitcast.9, s32[4,8]{1,0:T(4,128)} %bitcast.5, f32[4,8]{1,0:T(4,128)} %bitcast.6, bf16[2,128,1024]{2,1,0:T(8,128)(2,1)} %gate_hbm.1, ...), custom_call_target="tpu_custom_call" | custom-call | tf_op jit(solution)/shard_map/pallas_call | solution.py:436
  37.7 0.6 %copy.11 = bf16[8,128]{1,0:T(8,128)(2,1)} copy(bf16[8,128]{1,0:T(8,128)(2,1)S(1)} %shard_map.91) | data formatting | bytes 4096

commit v10 on v9

--- a/solution.py
+++ b/solution.py
@@ -97,7 +97,14 @@
         signal(barrier, {"ep": to * nx + x, "tp": tp})
 
     planes(z + 1, first + part, greet)
-    each(2 * nx, lambda k: signal(barrier, dev(dx=k // 2, dc=k % 2)))
+    go_x = [lax.rem(x + d, nx) for d in range(nx)]
+    go_tp = [tp, tp + 1 - 2 * c]
+
+    def mate(k):
+        return {"ep": z * nx + go_x[k // 2], "tp": go_tp[k % 2]}
+
+    for k in range(1, 2 * nx):
+        signal(barrier, mate(k))
 
     planes(rank + 1, ny, lambda r: signal(barrier, {"ep": ep, "tp": 2 * ranked(r) + c}))
 
@@ -137,15 +144,14 @@
         planes(part, nz, greet)
 
     def x_copy(k):
-        return remote(xt.at[0], xt.at[k], ssem.at[0], rsem.at[0], dev(dx=k // 2, dc=k % 2))
+        return remote(xt.at[0], xt.at[k], ssem.at[0], rsem.at[0], mate(k))
 
     def x_shares(dx):
-        return remote(xs.at[0], xs.at[dx], ssem.at[1], rsem.at[1], dev(dx=dx))
-
-    each(2 * nx, lambda k: x_copy(k).start())
-
-    go_x = [lax.rem(x + d, nx) for d in range(nx)]
-    go_tp = [tp, tp + 1 - 2 * c]
+        return remote(xs.at[0], xs.at[dx], ssem.at[1], rsem.at[1], mate(2 * dx))
+
+    for k in range(1, 2 * nx):
+        x_copy(k).start()
+
 
     def straight(to):
         for k in range(2 * nx):
@@ -181,7 +187,8 @@
         shares = shares + jnp.where(lane == pick, high, 0.0)
         shares = shares + jnp.where(lane == pick + EPG, low, 0.0)
     xs[0] = pack(shares).astype(BF16)
-    each(nx, lambda k: x_shares(k).start())
+    for dx in range(1, nx):
+        x_shares(dx).start()
 
     done(wgu.at[:, :, 0:L, :], lsem.at[0])
     done(gb, wsem.at[1])
@@ -288,9 +295,7 @@
             else:
                 ps[d - 1, 0, here] = gate_part.astype(BF16)
                 ps[d - 1, 1, here] = up_part.astype(BF16)
-                if place == 0:
-                    p_copy(b, d).start()
-                else:
+                if place:
                     waiting.append(d)
                 if place in (2, ny - 2):
 
@@ -307,7 +312,13 @@
                 columns = jnp.transpose(columns)
                 ax2s[b, :, 0:batch_rows] = columns[0:2, :]
                 ax2r[b, 0, :, 0:batch_rows] = columns[0:2, :]
-                each(ny, lambda d: a2_copy(b, d).start())
+
+                @pl.when(ep >= 0)
+                def _():
+                    for w in far_first(ny):
+                        a2_copy(b, w).start()
+                    p_copy(b, far_first(ny)[0]).start()
+
 
     def h_copy(b, d):
         here = rows_of(b)

time: 38.4 us -> 38 us (0.990)
  Pallas kernels: 37.7 us -> 37.2 us
    pallas_call x1, Pallas kernels: 37.7 us -> 37.2 us  [on_device(): pl.pallas_call(functools.partial(kernel, nz, nx, ny, width * 2 * ny), out...]
where the time goes in v10:
time: 38 us; the launch traced here: 37.8 us
  Pallas kernels  37.2 us (98%)
  local copies, waits for them, and re-layouts  0.58 us (2%)
    pallas_call x1, Pallas kernels, on_device(): pl.pallas_call(functools.partial(kernel, nz, nx, ny, width * 2 * ny), out...  37.2 us

profile of v10, /device:TPU:1, one launch (start us, length us, event | category | flops | bytes accessed | tf_op | source)
XLA Modules:
  0.0 37.8 jit_solution(498773771807480576)
XLA Ops:
  0.0 37.2 %shard_map.91 = bf16[8,128]{1,0:T(8,128)(2,1)S(1)} custom-call(bf16[8,128]{1,0:T(8,128)(2,1)} %tok_hbm.1, f32[1,128]{1,0:T(1,128)} %bitcast.7, f32[1,128]{1,0:T(1,128)} %bitcast.8, s32[1,8]{1,0:T(1,128)} %bitcast.9, s32[4,8]{1,0:T(4,128)} %bitcast.5, f32[4,8]{1,0:T(4,128)} %bitcast.6, bf16[2,128,1024]{2,1,0:T(8,128)(2,1)} %gate_hbm.1, ...), custom_call_target="tpu_custom_call" | custom-call | tf_op jit(solution)/shard_map/pallas_call | solution.py:447
  37.2 0.6 %copy.11 = bf16[8,128]{1,0:T(8,128)(2,1)} copy(bf16[8,128]{1,0:T(8,128)(2,1)S(1)} %shard_map.91) | data formatting | bytes 4096

commit v11 on v10

--- a/solution.py
+++ b/solution.py
@@ -31,8 +31,8 @@
     out_ref,
     tok_ref, gain_ref, bias_ref, gp_ref, mp_ref, pp_ref,
     wgu, wd, gb,
-    xt, xs, zs, tr, sr, ax1s, ax1r, ax2s, ax2r, ps, pr, hb, os, rr,
-    zready, yready, isem, lsem, wsem, ssem, rsem, tsem, asem, psem, hsem,
+    xt, xs, zs, tr, sr, halfway, ax1s, ax1r, ax2s, ax2r, ps, pr, hb, os, rr,
+    zready, yready, fsem, isem, lsem, wsem, ssem, rsem, tsem, asem, psem, hsem,
 ):
     tokens = tok_ref.shape[0]
     half = wgu.shape[3]
@@ -224,7 +224,26 @@
         z_copy(to)
 
     planes(first, z, z_copy)
-    planes(z + 1, nz, z_ready_copy)
+    planes(z + 1, first + part, z_ready_copy)
+    step = part // 2
+
+    @pl.when(z < step)
+    def _():
+        device = {"ep": (z + step) * nx + x, "tp": tp}
+        remote(xt.at[:, z + part], halfway, ssem.at[2], fsem.at[0], device).start()
+        planes(part, z + part, z_ready_copy)
+        planes(z + part + 1, nz, z_ready_copy)
+        pl.semaphore_wait(zready.at[z + part], 1)
+
+    @pl.when((z >= step) & (z < part))
+    def _():
+        pl.semaphore_wait(zready.at[z + step], 1)
+        done(halfway, fsem.at[0])
+        device = {"ep": (z + step) * nx + x, "tp": tp}
+        remote(halfway, tr.at[z - step], fsem.at[1], tsem.at[0], device).start()
+        z_copy(z + step)
+        planes(part, z + step, z_ready_copy)
+        planes(z + step + 1, nz, z_ready_copy)
 
     def z_shares(d):
         return remote(zs.at[lax.rem(z + d, nz)], sr.at[z], ssem.at[3], rsem.at[3], dev(dz=d))
@@ -407,6 +426,11 @@
     rr[z * 2 * nx] = os[z * 2 * nx]
 
     done(xt.at[pl.ds(1, 2 * nx - 1)], ssem.at[0])
+
+    @pl.when((z >= step) & (z < part))
+    def _():
+        done(halfway, fsem.at[1])
+
     done(xs.at[pl.ds(1, nx - 1)], ssem.at[1])
     done(tr.at[pl.ds(1, nz - 1)], ssem.at[2])
     done(sr.at[pl.ds(1, nz - 1)], ssem.at[3])
@@ -464,6 +488,7 @@
                 vmem((nz, nx * CAP, L), BF16),
                 vmem((nz, 2 * nx, CAP, L), BF16),
                 vmem((nz, nx * CAP, L), BF16),
+                vmem((2 * nx, CAP, L), BF16),
                 vmem((ny, 2, 2 * L), F32),
                 vmem((ny, 2, 2 * L), F32),
                 vmem((2, 2, L), F32),
@@ -475,6 +500,7 @@
                 vmem((2 * nx * nz, CAP, L), BF16),
                 pltpu.SemaphoreType.REGULAR((nz,)),
                 pltpu.SemaphoreType.REGULAR,
+                dma((2,)),
                 dma((6,)),
                 dma((2,)),
                 dma((6,)),

time: 38 us -> 37.8 us (level)
  no operation moved by 1% of the time
where the time goes in v11:
time: 37.8 us; the launch traced here: 37.7 us
  Pallas kernels  37.1 us (98%)
  local copies, waits for them, and re-layouts  0.58 us (2%)
    pallas_call x1, Pallas kernels, on_device(): pl.pallas_call(functools.partial(kernel, nz, nx, ny, width * 2 * ny), out...  37.1 us

profile of v11, /device:TPU:1, one launch (start us, length us, event | category | flops | bytes accessed | tf_op | source)
XLA Modules:
  0.0 37.7 jit_solution(11344264970740190866)
XLA Ops:
  0.0 37.1 %shard_map.91 = bf16[8,128]{1,0:T(8,128)(2,1)S(1)} custom-call(bf16[8,128]{1,0:T(8,128)(2,1)} %tok_hbm.1, f32[1,128]{1,0:T(1,128)} %bitcast.7, f32[1,128]{1,0:T(1,128)} %bitcast.8, s32[1,8]{1,0:T(1,128)} %bitcast.9, s32[4,8]{1,0:T(4,128)} %bitcast.5, f32[4,8]{1,0:T(4,128)} %bitcast.6, bf16[2,128,1024]{2,1,0:T(8,128)(2,1)} %gate_hbm.1, ...), custom_call_target="tpu_custom_call" | custom-call | tf_op jit(solution)/shard_map/pallas_call | solution.py:471
  37.1 0.6 %copy.11 = bf16[8,128]{1,0:T(8,128)(2,1)} copy(bf16[8,128]{1,0:T(8,128)(2,1)S(1)} %shard_map.91) | data formatting | bytes 4096

commit v12 on v11

--- a/solution.py
+++ b/solution.py
@@ -137,7 +137,6 @@
 
     pl.semaphore_wait(barrier, (2 * nx - 1) + z + rank)
     planes(0, z, lambda to: signal(zready.at[z], {"ep": to * nx + x, "tp": tp}))
-    planes(0, rank, lambda r: signal(yready, {"ep": ep, "tp": 2 * ranked(r) + c}))
 
     @pl.when(side == 0)
     def _():
@@ -151,6 +150,7 @@
 
     for k in range(1, 2 * nx):
         x_copy(k).start()
+    planes(0, rank, lambda r: signal(yready, {"ep": ep, "tp": 2 * ranked(r) + c}))
 
 
     def straight(to):

time: 37.8 us -> 37.8 us (level)
  no operation moved by 1% of the time
where the time goes in v12:
time: 37.8 us; the launch traced here: 37.7 us
  Pallas kernels  37.1 us (98%)
  local copies, waits for them, and re-layouts  0.58 us (2%)
    pallas_call x1, Pallas kernels, on_device(): pl.pallas_call(functools.partial(kernel, nz, nx, ny, width * 2 * ny), out...  37.1 us

profile of v12, /device:TPU:1, one launch (start us, length us, event | category | flops | bytes accessed | tf_op | source)
XLA Modules:
  0.0 37.7 jit_solution(6252378959222686057)
XLA Ops:
  0.0 37.1 %shard_map.91 = bf16[8,128]{1,0:T(8,128)(2,1)S(1)} custom-call(bf16[8,128]{1,0:T(8,128)(2,1)} %tok_hbm.1, f32[1,128]{1,0:T(1,128)} %bitcast.7, f32[1,128]{1,0:T(1,128)} %bitcast.8, s32[1,8]{1,0:T(1,128)} %bitcast.9, s32[4,8]{1,0:T(4,128)} %bitcast.5, f32[4,8]{1,0:T(4,128)} %bitcast.6, bf16[2,128,1024]{2,1,0:T(8,128)(2,1)} %gate_hbm.1, ...), custom_call_target="tpu_custom_call" | custom-call | tf_op jit(solution)/shard_map/pallas_call | solution.py:471
  37.1 0.6 %copy.11 = bf16[8,128]{1,0:T(8,128)(2,1)} copy(bf16[8,128]{1,0:T(8,128)(2,1)S(1)} %shard_map.91) | data formatting | bytes 4096

commit v13 on v12

--- a/solution.py
+++ b/solution.py
@@ -63,6 +63,33 @@
     def signal(sem, device):
         pl.semaphore_signal(sem, inc=1, device_id=device, device_id_type=MESH)
 
+    def planes(low, high, body):
+        lax.fori_loop(low, high, lambda to, carry: (body(to), carry)[1], 0)
+
+    part = nz // 2
+    side = z // part
+    first = side * part
+
+    def ranked(r):
+        return r + r // per_expert * (3 * per_expert - 1 - 2 * r)
+
+    rank = ranked(y)
+    own_batch = (z + nz - EARLY) // nz
+    barrier = pltpu.get_barrier_semaphore()
+
+    def greet(to):
+        signal(barrier, {"ep": to * nx + x, "tp": tp})
+
+    go_x = [lax.rem(x + d, nx) for d in range(nx)]
+    go_tp = [tp, tp + 1 - 2 * c]
+
+    def mate(k):
+        return {"ep": z * nx + go_x[k // 2], "tp": go_tp[k % 2]}
+
+    for k in range(1, 2 * nx):
+        signal(barrier, mate(k))
+
+    planes(z + 1, first + part, greet)
     inputs = [
         pltpu.make_async_copy(src, dst, isem.at[i])
         for i, (src, dst) in enumerate(
@@ -78,33 +105,6 @@
     ]
     for copy in inputs:
         copy.start()
-
-    def planes(low, high, body):
-        lax.fori_loop(low, high, lambda to, carry: (body(to), carry)[1], 0)
-
-    part = nz // 2
-    side = z // part
-    first = side * part
-
-    def ranked(r):
-        return r + r // per_expert * (3 * per_expert - 1 - 2 * r)
-
-    rank = ranked(y)
-    own_batch = (z + nz - EARLY) // nz
-    barrier = pltpu.get_barrier_semaphore()
-
-    def greet(to):
-        signal(barrier, {"ep": to * nx + x, "tp": tp})
-
-    planes(z + 1, first + part, greet)
-    go_x = [lax.rem(x + d, nx) for d in range(nx)]
-    go_tp = [tp, tp + 1 - 2 * c]
-
-    def mate(k):
-        return {"ep": z * nx + go_x[k // 2], "tp": go_tp[k % 2]}
-
-    for k in range(1, 2 * nx):
-        signal(barrier, mate(k))
 
     planes(rank + 1, ny, lambda r: signal(barrier, {"ep": ep, "tp": 2 * ranked(r) + c}))
 

time: 37.8 us -> 37.8 us (level)
  no operation moved by 1% of the time
where the time goes in v13:
time: 37.8 us; the launch traced here: 37.7 us
  Pallas kernels  37.1 us (98%)
  local copies, waits for them, and re-layouts  0.58 us (2%)
    pallas_call x1, Pallas kernels, on_device(): pl.pallas_call(functools.partial(kernel, nz, nx, ny, width * 2 * ny), out...  37.1 us

profile of v13, /device:TPU:1, one launch (start us, length us, event | category | flops | bytes accessed | tf_op | source)
XLA Modules:
  0.0 37.7 jit_solution(3923115132907213936)
XLA Ops:
  0.0 37.1 %shard_map.91 = bf16[8,128]{1,0:T(8,128)(2,1)S(1)} custom-call(bf16[8,128]{1,0:T(8,128)(2,1)} %tok_hbm.1, f32[1,128]{1,0:T(1,128)} %bitcast.7, f32[1,128]{1,0:T(1,128)} %bitcast.8, s32[1,8]{1,0:T(1,128)} %bitcast.9, s32[4,8]{1,0:T(4,128)} %bitcast.5, f32[4,8]{1,0:T(4,128)} %bitcast.6, bf16[2,128,1024]{2,1,0:T(8,128)(2,1)} %gate_hbm.1, ...), custom_call_target="tpu_custom_call" | custom-call | tf_op jit(solution)/shard_map/pallas_call | solution.py:471
  37.1 0.6 %copy.11 = bf16[8,128]{1,0:T(8,128)(2,1)} copy(bf16[8,128]{1,0:T(8,128)(2,1)S(1)} %shard_map.91) | data formatting | bytes 4096

commit v14 on v13

--- a/solution.py
+++ b/solution.py
@@ -316,7 +316,7 @@
                 ps[d - 1, 1, here] = up_part.astype(BF16)
                 if place:
                     waiting.append(d)
-                if place in (2, ny - 2):
+                if place in (2, 4, ny - 2):
 
                     @pl.when(ep >= 0)
                     def _():

time: 37.8 us -> 37.7 us (level)
  no operation moved by 1% of the time
where the time goes in v14:
time: 37.7 us; the launch traced here: 37.6 us
  Pallas kernels  37 us (98%)
  local copies, waits for them, and re-layouts  0.58 us (2%)
    pallas_call x1, Pallas kernels, on_device(): pl.pallas_call(functools.partial(kernel, nz, nx, ny, width * 2 * ny), out...  37 us

profile of v14, /device:TPU:1, one launch (start us, length us, event | category | flops | bytes accessed | tf_op | source)
XLA Modules:
  0.0 37.6 jit_solution(2229786338318194087)
XLA Ops:
  0.0 37.0 %shard_map.91 = bf16[8,128]{1,0:T(8,128)(2,1)S(1)} custom-call(bf16[8,128]{1,0:T(8,128)(2,1)} %tok_hbm.1, f32[1,128]{1,0:T(1,128)} %bitcast.7, f32[1,128]{1,0:T(1,128)} %bitcast.8, s32[1,8]{1,0:T(1,128)} %bitcast.9, s32[4,8]{1,0:T(4,128)} %bitcast.5, f32[4,8]{1,0:T(4,128)} %bitcast.6, bf16[2,128,1024]{2,1,0:T(8,128)(2,1)} %gate_hbm.1, ...), custom_call_target="tpu_custom_call" | custom-call | tf_op jit(solution)/shard_map/pallas_call | solution.py:471
  37.0 0.6 %copy.11 = bf16[8,128]{1,0:T(8,128)(2,1)} copy(bf16[8,128]{1,0:T(8,128)(2,1)S(1)} %shard_map.91) | data formatting | bytes 4096
